TPU v7x, 32 devices: a whole 2x2x4 slice. The times are simulated.
32 devices in a mesh: kv: 16 (over z, y, x), tp: 2 (over core).
Axes of the slice: x: 2, y: 2, z: 4, core: 2. Of those that a mesh axis runs over, the one named last changes fastest.
Arguments:
- normed: bfloat16 [8192, 4096], P('kv'), may hold values from -6 to 6
- queries: bfloat16 [8192, 1024], P('kv', 'tp'), may hold values from -6 to 6
- keys: bfloat16 [8192, 64], P('kv'), may hold values from -6 to 6
- values: bfloat16 [8192, 64], P('kv'), may hold values from -6 to 6
- attended: bfloat16 [8192, 1024], P('kv', 'tp'), may hold values from -6 to 6
- cotangent: bfloat16 [8192, 1024], P('kv', 'tp'), may hold values from -24 to 24
- log_sum: float32 [8192, 16], P('kv', 'tp'), may hold values from 6 to 8
- chosen: int32 [128, 16], P('kv'), may hold values from -1 to 127, as said below
Outputs:
- grad_queries: bfloat16 [8192, 1024], P('kv', 'tp')
- grad_keys: float32 [8192, 64], P('kv')
- grad_values: float32 [8192, 64], P('kv')
- weight_grad: float32 [4096, 1024], P('kv', 'tp')
Inputs may be any that keep to these rules, and one draw needn't show every extreme that they name: `chosen`: each row lists distinct key blocks, none after its own block, and always its own block; the listed entries come first and -1 fills the rest. A row lists from 8 to 16 blocks, fewer only where fewer blocks are open to it; on every index of kv some row lists 16 blocks where that many are open. The rows of one index of kv together list at most one block of each other index of kv's positions; every index of kv from 1 on lists a block of index 0 and a block of the index before it, and every index from half the axis on a block of the index half the axis before it.
All inputs are finite; a program needn't handle non-finite values.
Results may differ from a plain program's by a relative error of at most 0.007.
Values may be sent and summed in bfloat16 or wider, within the bound.
No kernel may reach another device: no remote copies, remote signals or barrier semaphores. Data moves between devices by JAX's collectives and lax.ppermute only.
A program may use at most 64 MiB of HBM per device.

v0:
```python
import functools
import math

import jax
import jax.numpy as jnp
from jax import lax
from jax.experimental import pallas as pl
from jax.experimental.pallas import tpu as pltpu

from jax.sharding import PartitionSpec as P

BLOCK = 64
STACK_UNROLL = 4
BLOCK_UNROLL = 2


def flat_perm(kv_of, tp_of=lambda core: core):
    kv_size, tp_size = lax.axis_size("kv"), lax.axis_size("tp")
    return [
        (kv * tp_size + tp, kv_of(kv) * tp_size + tp_of(tp))
        for kv in range(kv_size)
        for tp in range(tp_size)
    ]


def send(value, perm):
    return lax.ppermute(value, ("kv", "tp"), perm)


def group_size():
    kv_size = lax.axis_size("kv")
    return 4 if kv_size % 4 == 0 else 2 if kv_size % 2 == 0 else 1


def step_perm(step, size, stride):
    if size & (size - 1) == 0:
        return lambda kv: kv ^ (step * stride)
    base = size * stride
    return lambda kv: kv // base * base + (kv % base + step * stride) % base


def partner(index, step, size):
    return index ^ step if size & (size - 1) == 0 else (index + step) % size


def columns_of(normed, member, group, first, rows):
    kv_size = lax.axis_size("kv")
    width = normed.shape[1] // kv_size
    parts = [
        lax.dynamic_slice(normed, (first, (outer * group + member) * width), (rows, width))
        for outer in range(kv_size // group)
    ]
    return jnp.concatenate(parts, axis=1)


def regroup_normed(normed, share):
    group = group_size()
    member = lax.axis_index("kv") % group
    half = normed.shape[0] // 2
    pieces = [
        columns_of(normed, partner(member, step, group), group, share * half, half)
        for step in range(1, group)
    ]
    mine = [
        columns_of(normed, member, group, first * half, half) for first in (share, 1 - share)
    ]
    return pieces, jnp.concatenate(mine, axis=0)


def exchange_normed(pieces):
    group = group_size()
    got = [
        send(piece, flat_perm(step_perm(step, group, 1)))
        for step, piece in enumerate(pieces, start=1)
    ]
    other = send(jnp.stack(got), flat_perm(lambda kv: kv, lambda tp: tp ^ 1))
    return got, other


def gather_group(value):
    group = group_size()
    return [send(value, flat_perm(step_perm(step, group, 1))) for step in range(1, group)]


def plane_kernel(outer, group, place_ref, *refs):
    rights, mine_ref, others = refs[:group], refs[group], refs[group + 1:2 * group]
    other_ref, own_ref, pieces = refs[2 * group], refs[2 * group + 1], refs[2 * group + 2:]
    half = mine_ref.shape[0] // 2
    width = mine_ref.shape[1] // outer
    for step in range(outer):
        owner = partner(place_ref[0], step, outer)
        columns = pl.ds(pl.multiple_of(owner * width, width), width)
        total = jnp.dot(
            rights[0][...], mine_ref[:, columns], preferred_element_type=jnp.float32
        )
        for i in range(group - 1):
            total += jnp.dot(
                rights[i + 1][:, :half], others[i][:, columns],
                preferred_element_type=jnp.float32,
            )
            total += jnp.dot(
                rights[i + 1][:, half:], other_ref[i, :, columns],
                preferred_element_type=jnp.float32,
            )
        if step == 0:
            own_ref[...] = total
        else:
            pieces[step - 1][...] = total.astype(jnp.bfloat16)


def weight_gradient(mine, got, other, rights):
    group = group_size()
    outer = lax.axis_size("kv") // group
    place = lax.axis_index("kv") // group
    columns = rights[0].shape[0]
    width = mine.shape[1] // outer
    if width % 128 == 0:
        in_vmem = pl.BlockSpec(memory_space=pltpu.VMEM)
        own, *pieces = pl.pallas_call(
            functools.partial(plane_kernel, outer, group),
            in_specs=[pl.BlockSpec(memory_space=pltpu.SMEM)] + [in_vmem] * (2 * group + 1),
            out_specs=[in_vmem] * outer,
            out_shape=[jax.ShapeDtypeStruct((columns, width), jnp.float32)] + [
                jax.ShapeDtypeStruct((columns, width), jnp.bfloat16)
            ] * (outer - 1),
            cost_estimate=pl.CostEstimate(
                flops=2 * columns * mine.size * group,
                bytes_accessed=2 * group * mine.size,
                transcendentals=0,
            ),
        )(place.reshape(1).astype(jnp.int32), *rights, mine, *got, other)
    else:
        lefts = [mine]
        for i, piece in enumerate(got):
            lefts += [piece, other[i]]
        partial = jnp.dot(
            jnp.concatenate(rights, axis=1), jnp.concatenate(lefts, axis=0),
            preferred_element_type=jnp.float32,
        )
        own, *pieces = [
            lax.dynamic_slice_in_dim(partial, partner(place, step, outer) * width, width, axis=1)
            for step in range(outer)
        ]
        pieces = [piece.astype(jnp.bfloat16) for piece in pieces]
    terms = [own]
    for step, piece in enumerate(pieces, start=1):
        terms.append(send(piece, flat_perm(step_perm(step, outer, group))))
    return terms


def sum_over_tp(value):
    tp_size = lax.axis_size("tp")
    step = 1
    if tp_size & (tp_size - 1):
        return lax.psum(value, "tp")
    while step < tp_size:
        value = value + send(value, flat_perm(lambda kv: kv, lambda tp: tp ^ step))
        step *= 2
    return value


def attention_kernel(
    head_dim, first, last, part, share_ref, slot_ref, limit_ref, q_ref, d_ref, log_ref, sum_ref,
    table_ref, *rest,
):
    before_ref = None if first else rest[0]
    dq_ref, turned_ref, sums_ref, stack_ref, dq_t_ref, lse_ref, delta_ref = rest[-7:]
    blocks, slot_count = slot_ref.shape
    width = lse_ref.shape[2]
    half = width // 2
    wide = 2 * head_dim
    pairs = width // (2 * BLOCK)
    offset = part * pairs
    score_scale = head_dim ** (-0.5)
    low = lax.broadcasted_iota(jnp.int32, (BLOCK, wide), 1) < head_dim

    sums_ref[...] = jnp.zeros_like(sums_ref) if first else before_ref[...]

    def stack_heads(block, carry):
        rows = pl.ds(pl.multiple_of(block * BLOCK, BLOCK), BLOCK)
        for pair in range(pairs):
            columns = pl.ds((offset + pair) * wide, wide)
            query = q_ref[rows, columns].astype(jnp.float32)
            grad = d_ref[rows, columns].astype(jnp.float32)
            turned = pltpu.roll(query, head_dim, 1)
            turned_grad = pltpu.roll(grad, head_dim, 1)
            for place, value in enumerate((
                jnp.where(low, query, 0.0), jnp.where(low, turned, 0.0),
                jnp.where(low, 0.0, turned_grad), jnp.where(low, 0.0, grad),
            )):
                stack_ref[block, pl.ds((place * pairs + pair) * BLOCK, BLOCK), :] = value.astype(
                    jnp.bfloat16
                )
        return carry

    lax.fori_loop(0, blocks, stack_heads, 0, unroll=min(blocks, STACK_UNROLL))
    for block in range(blocks):
        rows = slice(block * BLOCK, (block + 1) * BLOCK)
        for parity in range(2):
            for pair in range(pairs):
                head = 2 * (offset + pair) + parity
                place = slice((parity * pairs + pair) * BLOCK, (parity * pairs + pair + 1) * BLOCK)
                lse_ref[block, :, place] = log_ref[head:head + 1, rows] * math.log2(math.e)
                delta_ref[block, :, place] = sum_ref[head:head + 1, rows]
    shape = (BLOCK, width)
    ahead = lax.broadcasted_iota(jnp.int32, shape, 0) - (
        lax.broadcasted_iota(jnp.int32, shape, 1) & (BLOCK - 1)
    )

    def one_block(block, carry):
        stack = stack_ref[block]
        places = [slot_ref[block, i] for i in range(slot_count)]
        limits = [limit_ref[block, i] for i in range(slot_count)]
        rows = [pl.ds(pl.multiple_of(place * BLOCK, BLOCK), BLOCK) for place in places]
        pair_rows = jnp.concatenate([table_ref[row, :] for row in rows], axis=0)
        both = lax.dot_general(
            pair_rows, stack, (((1,), (1,)), ((), ())), preferred_element_type=jnp.float32
        )
        allowed = jnp.concatenate([ahead <= limit for limit in limits], axis=0)
        powers = both[:, :width] * (score_scale * math.log2(math.e)) - lse_ref[block]
        probs = jnp.where(allowed, jnp.exp2(powers), 0.0)
        dscores = (probs * (both[:, width:] - delta_ref[block])).astype(jnp.bfloat16)
        terms = jnp.concatenate([dscores, probs.astype(jnp.bfloat16)], axis=1)
        grads = jnp.dot(terms, stack, preferred_element_type=jnp.float32)
        dq_t_ref[block] = score_scale * lax.dot_general(
            pair_rows[:, :head_dim], dscores, (((0,), (0,)), ((), ())),
            preferred_element_type=jnp.float32,
        )
        for i, row in enumerate(rows):
            sums_ref[row, :] += grads[i * BLOCK:(i + 1) * BLOCK]
        return carry

    lax.fori_loop(0, blocks, one_block, 0, unroll=BLOCK_UNROLL)

    def write_two(turn, carry):
        first_block = 2 * turn
        to = lax.rem(first_block + share_ref[0] * (blocks // 2), blocks) * BLOCK
        for pair in range(pairs):
            cols = slice(pair * BLOCK, (pair + 1) * BLOCK)
            odd_cols = slice(half + pair * BLOCK, half + (pair + 1) * BLOCK)
            heads_t = []
            for block in (first_block, first_block + 1):
                heads_t.append(jnp.concatenate(
                    [dq_t_ref[block, :, cols], dq_t_ref[block, :, odd_cols]], axis=0
                ))
            both_t = jnp.concatenate(heads_t, axis=1)
            turned_ref[pl.ds(pair * wide, wide), pl.ds(pl.multiple_of(to, 2 * BLOCK), 2 * BLOCK)] = (
                both_t.astype(jnp.bfloat16)
            )
            dq_ref[
                pl.ds(pl.multiple_of(first_block * BLOCK, 2 * BLOCK), 2 * BLOCK),
                pl.ds(pair * wide, wide),
            ] = both_t.T.astype(jnp.bfloat16)
        return carry

    lax.fori_loop(0, blocks // 2, write_two, 0, unroll=min(blocks // 2, STACK_UNROLL))
    if last:
        sums = sums_ref[...]
        low_columns = lax.broadcasted_iota(jnp.int32, sums.shape, 1) < head_dim
        sums_ref[...] = jnp.where(low_columns, sums * score_scale, sums)


def attention_backward(
    queries, cotangent, log_sum, deltas, table, share, slot_index, limits, part, parts, before
):
    tok_rows, width = queries.shape
    blocks, slot_count = slot_index.shape
    head_dim = table.shape[1] // 2
    width //= parts
    heads = width // head_dim
    first, last = part == 0, part == parts - 1
    in_smem = pl.BlockSpec(memory_space=pltpu.SMEM)
    in_vmem = pl.BlockSpec(memory_space=pltpu.VMEM)
    return pl.pallas_call(
        functools.partial(attention_kernel, head_dim, first, last, part),
        in_specs=[in_smem] * 3 + [in_vmem] * (5 if first else 6),
        out_specs=[in_vmem] * 3,
        scratch_shapes=[
            pltpu.VMEM((blocks, 2 * heads * BLOCK, 2 * head_dim), jnp.bfloat16),
            pltpu.VMEM((blocks, head_dim, heads * BLOCK), jnp.float32),
            pltpu.VMEM((blocks, 1, heads * BLOCK), jnp.float32),
            pltpu.VMEM((blocks, 1, heads * BLOCK), jnp.float32),
        ],
        out_shape=[
            jax.ShapeDtypeStruct((tok_rows, width), jnp.bfloat16),
            jax.ShapeDtypeStruct((width, tok_rows), jnp.bfloat16),
            jax.ShapeDtypeStruct(table.shape, jnp.float32),
        ],
        cost_estimate=pl.CostEstimate(
            flops=10 * tok_rows * slot_count * BLOCK * width,
            bytes_accessed=4 * tok_rows * width * 2,
            transcendentals=tok_rows * heads * slot_count * BLOCK,
        ),
    )(
        share.reshape(1), slot_index, limits, queries, cotangent, log_sum, deltas, table,
        *(() if first else (before,)),
    )


def shards(normed, queries, keys, values, attended, cotangent, log_sum, chosen):
    my_rank = lax.axis_index("kv")
    peer_count = lax.axis_size("kv")
    tok_rows = normed.shape[0]
    local_blocks = tok_rows // BLOCK
    head_dim = keys.shape[1]
    pairs_local = jnp.concatenate([keys, values], axis=1).reshape(local_blocks, BLOCK, 2 * head_dim)
    owners = chosen // local_blocks
    within = chosen % local_blocks
    listed = chosen >= 0
    remote = listed & (owners != my_rank)
    peer_ids = jnp.arange(peer_count, dtype=jnp.int32)
    matched = remote[:, :, None] & (owners[:, :, None] == peer_ids[None, None, :])
    wanted = jnp.max(jnp.where(matched, within[:, :, None] + 1, 0), axis=(0, 1))
    asked_for = (
        lax.all_to_all(
            wanted.reshape(peer_count, 1), "kv", split_axis=0, concat_axis=0, tiled=True
        )[:, 0]
        - 1
    )
    picked = jnp.maximum(asked_for, 0)
    outgoing = jnp.take(pairs_local, picked, axis=0)
    outgoing, normed = lax.optimization_barrier((outgoing, normed))
    fetched = lax.all_to_all(outgoing, "kv", split_axis=0, concat_axis=0, tiled=True)
    share = (lax.axis_index("tp") % 2).astype(jnp.int32)
    pieces, mine = regroup_normed(normed, share)
    got, other = exchange_normed(pieces)
    block_table = jnp.concatenate([pairs_local, fetched], axis=0)
    slot_index = jnp.where(owners == my_rank, within, local_blocks + owners)
    slot_index = jnp.where(listed, slot_index, 0)
    heads = log_sum.shape[1]
    parts = 2 if heads % 4 == 0 else 1
    own = my_rank * local_blocks + jnp.arange(local_blocks, dtype=jnp.int32)
    limits = jnp.where(listed, (own[:, None] - chosen) * BLOCK, -BLOCK)
    head_of = jnp.arange(heads * head_dim, dtype=jnp.int32) // head_dim
    deltas = lax.dot_general(
        (jnp.arange(heads, dtype=jnp.int32)[:, None] == head_of[None, :]).astype(jnp.float32),
        cotangent.astype(jnp.float32) * attended.astype(jnp.float32),
        (((1,), (1,)), ((), ())), precision=lax.Precision.HIGHEST,
    )
    table = block_table.reshape(-1, 2 * head_dim)
    sums = None
    gradients, rights = [], []
    for part in range(parts):
        gradient, turned, sums = attention_backward(
            queries, cotangent, log_sum.T, deltas, table, share, slot_index, limits, part,
            parts, sums,
        )
        gradients.append(gradient)
        rights.append([turned] + gather_group(turned))
    query_gradient = jnp.concatenate(gradients, axis=1)
    block_sums = sums.reshape(block_table.shape)
    own_part = block_sums[:local_blocks]
    sent_back = block_sums[local_blocks:].astype(jnp.bfloat16)
    taken_by = (asked_for[:, None] == jnp.arange(local_blocks, dtype=jnp.int32)[None, :]).astype(
        jnp.float32
    )
    terms = [weight_gradient(mine, got, other, right) for right in rights]
    weight_grad = jnp.concatenate(
        [sum(term.astype(jnp.float32) for term in some) for some in terms], axis=0
    ).T
    returned = lax.all_to_all(sent_back, "kv", split_axis=0, concat_axis=0, tiled=True)
    totals = own_part + jnp.einsum(
        "sb,skc->bkc", taken_by, returned.astype(jnp.float32), precision=lax.Precision.HIGHEST
    )
    totals = sum_over_tp(totals)
    grad_keys = totals[:, :, :head_dim].reshape(tok_rows, head_dim)
    grad_values = totals[:, :, head_dim:].reshape(tok_rows, head_dim)
    return (query_gradient, grad_keys, grad_values, weight_grad)


def solution(mesh):
    placed = (
        P("kv", None),
        P("kv", "tp"),
        P("kv", None),
        P("kv", None),
        P("kv", "tp"),
        P("kv", "tp"),
        P("kv", "tp"),
        P("kv", None),
    )
    return jax.shard_map(
        shards,
        mesh=mesh,
        in_specs=placed,
        out_specs=(P("kv", "tp"), P("kv", None), P("kv", None), P("kv", "tp")),
        check_vma=False,
    )
```

profile of v0, /device:TPU:10, one launch (start us, length us, event | category | flops | bytes accessed | tf_op | source)
XLA Modules:
  0.0 134.7 jit_solution(14211725637103796757)
XLA Ops:
  0.6 0.7 compare_and_fusion
  1.4 1.4 %broadcast_add_fusion = (s32[8,16]{1,0:T(8,128)S(1)}, s32[8,16]{1,0:T(8,128)}, s32[8,16]{1,0:T(8,128)}) fusion(s32[8,16]{1,0:T(8,128)} %param.15, s32[8]{0:T(128)S(1)} %iota_add_fusion, s32[8,16]{1,0:T(8,128)S(1)} %get-tuple-element.59, s32[]{:T(128)S(6)} %axis_index.17), kind=kLoop, calls=%fused_computation.48 | loop fusion | flops 2560 | bytes 2596 | tf_op jit(solution)/shard_map/add | solution.py:313
  2.7 0.1 select_reduce_fusion
  2.8 0.7 copy.41
  3.5 7.2 %all-to-all-start = ((s32[16,1,1]{2,1,0:T(1,128)}), s32[16,1,1]{2,1,0:T(1,128)S(1)}, u32[]{:S(2)}, u32[]{:S(2)}) async-start(s32[16,1,1]{2,1,0:T(1,128)} %copy.41), calls=%async_computation | async-start | bytes 16384 | tf_op jit(solution)/shard_map/all_to_all | solution.py:315
  10.7 1.0 copy.39
  11.7 1.0 copy.40
  12.7 0.1 pad_maximum_fusion.6
  12.9 2.8 %all-to-all-done = s32[16,1,1]{2,1,0:T(1,128)S(1)} async-done(((s32[16,1,1]{2,1,0:T(1,128)}), s32[16,1,1]{2,1,0:T(1,128)S(1)}, u32[]{:S(2)}, u32[]{:S(2)}) %all-to-all-start) | async-done | bytes 96 | tf_op jit(solution)/shard_map/all_to_all | solution.py:315
  15.7 0.7 add_reduce_fusion
  16.4 0.6 gather_fusion
  17.0 0.8 broadcast_select_fusion
  17.8 2.8 %fusion.15 = (bf16[256,256]{1,0:T(8,128)(2,1)S(1)}, bf16[256,256]{1,0:T(8,128)(2,1)S(1)}, bf16[256,256]{1,0:T(8,128)(2,1)S(1)}, bf16[256,256]{1,0:T(8,128)(2,1)S...) fusion(bf16[512,4096]{1,0:T(8,128)(2,1)} %param.8, ...), kind=kLoop, calls=%fused_computation.53 | loop fusion | bytes 5242952 | tf_op jit(solution)/shard_map/dynamic_slice | solution.py:50
  20.7 1.5 %collective-permute-start.6 = (bf16[256,1024]{1,0:T(8,128)(2,1)S(1)}, bf16[256,1024]{1,0:T(8,128)(2,1)S(1)}, u32[]{:S(2)}, u32[]{:S(2)}) collective-permute-start(bf16[256,1024]{1,0:T(8,128)(2,1)S(1)} %pad_maximum_fusion.4), channel_id=1, source_target_pairs={{0,6},{1,7},{2,4},{3,5},{4,2},{5,3},{6,0},{7,1},{8,14},{9,15},{10,... | collective-permute-start | bytes 1572872 | tf_op jit(solution)/shard_map/ppermute | solution.py:27
  22.2 0.9 pad_maximum_fusion.3
  23.1 1.5 %collective-permute-start.5 = (bf16[256,1024]{1,0:T(8,128)(2,1)}, bf16[256,1024]{1,0:T(8,128)(2,1)S(1)}, u32[]{:S(2)}, u32[]{:S(2)}) collective-permute-start(bf16[256,1024]{1,0:T(8,128)(2,1)} %pad_maximum_fusion.3), channel_id=1, source_target_pairs={{0,4},{1,5},{2,6},{3,7},{4,0},{5,1},{6,2},{7,3},{8,12},{9,13},{10,... | collective-permute-start | bytes 1572872 | tf_op jit(solution)/shard_map/ppermute | solution.py:27
  24.5 0.9 pad_maximum_fusion.2
  25.4 0.6 collective-permute-start.4
  25.9 5.7 %all-to-all-start.1 = ((bf16[16,64,128]{2,1,0:T(8,128)(2,1)}), bf16[16,64,128]{2,1,0:T(8,128)(2,1)S(1)}, u32[]{:S(2)}, u32[]{:S(2)}) async-start(bf16[16,64,128]{2,1,0:T(8,128)(2,1)} %broadcast_select_fusion), calls=%async_computation.1 | async-start | bytes 524288 | tf_op jit(solution)/shard_map/all_to_all | solution.py:323
  31.7 1.3 fusion.sum_ref
  33.0 5.6 %collective-permute-done.6.refs_7_ = bf16[256,1024]{1,0:T(8,128)(2,1)S(1)} collective-permute-done((bf16[256,1024]{1,0:T(8,128)(2,1)S(1)}, bf16[256,1024]{1,0:T(8,128)(2,1)S(1)}, u32[]{:S(2)}, u32[]{:S(2)}) %collective-permute-start.6) | collective-permute-done | bytes 524320 | tf_op jit(solution)/shard_map/ppermute | solution.py:27
  38.6 8.9 %collective-permute-done.5.refs_6_ = bf16[256,1024]{1,0:T(8,128)(2,1)S(1)} collective-permute-done((bf16[256,1024]{1,0:T(8,128)(2,1)}, bf16[256,1024]{1,0:T(8,128)(2,1)S(1)}, u32[]{:S(2)}, u32[]{:S(2)}) %collective-permute-start.5) | collective-permute-done | bytes 524320 | tf_op jit(solution)/shard_map/ppermute | solution.py:27
  47.5 1.5 %pad_maximum_fusion = bf16[3,256,1024]{2,1,0:T(8,128)(2,1)} fusion(bf16[1,256,1024]{2,1,0:T(8,128)(2,1)S(1)} %bitcast.20, bf16[1,256,1024]{2,1,0:T(8,128)(2,1)S(1)} %bitcast.21, bf16[1,256,1024]{2,1,0:T(8,128)(2,1)S(1)} %bitcast.22), kind=kLoop, calls=%fused_computation.1 | loop fusion | flops 1572864 | bytes 3145728 | tf_op jit(solution)/shard_map/stack | solution.py:76
  49.0 0.8 pad_maximum_fusion.5
  49.8 9.0 %shard_map.111 = (bf16[512,256]{1,0:T(8,128)(2,1)}, bf16[256,512]{1,0:T(8,128)(2,1)}, f32[1536,128]{1,0:T(8,128)}) custom-call(s32[1]{0:T(128)} %bitcast.share_ref, s32[8,16]{1,0:T(8,128)} %get-tuple-element.84.slot_ref, s32[8,16]{1,0:T(8,128)} %get-tuple-element.83.limit_ref, bf16[512,512]{1,0:T(8,128)(2,1)} %q_ref.3, bf16[512,512]{1,0:T(8,128)(2,1)} %d_ref.3, ...), custom_call_target="tpu_custom_call" | custom-call | flops 1342177280 | bytes 1048576 | tf_op jit(solution)/shard_map/pallas_call | solution.py:274
  58.7 9.3 %shard_map.112 = (bf16[512,256]{1,0:T(8,128)(2,1)}, bf16[256,512]{1,0:T(8,128)(2,1)}, f32[1536,128]{1,0:T(8,128)}) custom-call(s32[1]{0:T(128)} %bitcast.share_ref, s32[8,16]{1,0:T(8,128)} %get-tuple-element.84.slot_ref, s32[8,16]{1,0:T(8,128)} %get-tuple-element.83.limit_ref, bf16[512,512]{1,0:T(8,128)(2,1)} %q_ref.3, bf16[512,512]{1,0:T(8,128)(2,1)} %d_ref.3, ...), custom_call_target="tpu_custom_call" | custom-call | flops 1342177280 | bytes 1048576 | tf_op jit(solution)/shard_map/pallas_call | solution.py:274
  68.1 1.9 %slice.28 = bf16[1024,128]{1,0:T(8,128)(2,1)} slice(f32[1536,128]{1,0:T(8,128)} %get-tuple-element.24), slice={[512:1536], [0:128]} | slice | bytes 524288 | tf_op jit(solution)/shard_map/slice | solution.py:353
  70.0 5.7 %all-to-all-start.2 = ((bf16[16,64,128]{2,1,0:T(8,128)(2,1)}), bf16[16,64,128]{2,1,0:T(8,128)(2,1)S(1)}, u32[]{:S(2)}, u32[]{:S(2)}) async-start(bf16[16,64,128]{2,1,0:T(8,128)(2,1)} %bitcast.7), calls=%async_computation.2 | async-start | bytes 524288 | tf_op jit(solution)/shard_map/all_to_all | solution.py:361
  75.7 1.0 slice.17
  76.6 8.1 %all-to-all-done.2 = bf16[16,64,128]{2,1,0:T(8,128)(2,1)S(1)} async-done(((bf16[16,64,128]{2,1,0:T(8,128)(2,1)}), bf16[16,64,128]{2,1,0:T(8,128)(2,1)S(1)}, u32[]{:S(2)}, u32[]{:S(2)}) %all-to-all-start.2) | async-done | bytes 262176 | tf_op jit(solution)/shard_map/all_to_all | solution.py:361
  84.8 0.3 convolution_add_fusion
  85.1 0.1 collective-permute-start
  85.2 1.5 %collective-permute-start.1 = (bf16[256,512]{1,0:T(8,128)(2,1)}, bf16[256,512]{1,0:T(8,128)(2,1)S(1)}, u32[]{:S(2)}, u32[]{:S(2)}) collective-permute-start(bf16[256,512]{1,0:T(8,128)(2,1)} %get-tuple-element.25.refs_0_), channel_id=1, source_target_pairs={{0,2},{1,3},{2,0},{3,1},{4,6},{5,7},{6,4},{7,5},{8,10},{9,11},{10,... | collective-permute-start | bytes 786440 | tf_op jit(solution)/shard_map/ppermute | solution.py:27
  86.7 0.7 collective-permute-start.2
  87.4 1.3 collective-permute-start.3
  88.7 1.5 %collective-permute-start.11 = (bf16[256,512]{1,0:T(8,128)(2,1)}, bf16[256,512]{1,0:T(8,128)(2,1)}, u32[]{:S(2)}, u32[]{:S(2)}) collective-permute-start(bf16[256,512]{1,0:T(8,128)(2,1)} %get-tuple-element.31.refs_0_), channel_id=1, source_target_pairs={{0,2},{1,3},{2,0},{3,1},{4,6},{5,7},{6,4},{7,5},{8,10},{9,11},{10,... | collective-permute-start | bytes 786440 | tf_op jit(solution)/shard_map/ppermute | solution.py:27
  90.2 1.1 maximum_maximum_fusion.refs_4_
  91.4 1.9 %pad_maximum_fusion.1 = bf16[512,512]{1,0:T(8,128)(2,1)} fusion(bf16[512,256]{1,0:T(8,128)(2,1)} %get-tuple-element.23, bf16[512,256]{1,0:T(8,128)(2,1)} %get-tuple-element.21), kind=kLoop, calls=%fused_computation.9 | loop fusion | flops 1048576 | bytes 1048576 | tf_op jit(solution)/shard_map/concatenate | solution.py:350
  93.3 1.4 %collective-permute-done.1.refs_1_ = bf16[256,512]{1,0:T(8,128)(2,1)S(1)} collective-permute-done((bf16[256,512]{1,0:T(8,128)(2,1)}, bf16[256,512]{1,0:T(8,128)(2,1)S(1)}, u32[]{:S(2)}, u32[]{:S(2)}) %collective-permute-start.1) | collective-permute-done | bytes 262176 | tf_op jit(solution)/shard_map/ppermute | solution.py:27
  94.6 0.7 collective-permute-start.12
  95.4 6.3 %collective-permute-done.2.refs_2_ = bf16[256,512]{1,0:T(8,128)(2,1)S(1)} collective-permute-done((bf16[256,512]{1,0:T(8,128)(2,1)}, bf16[256,512]{1,0:T(8,128)(2,1)S(1)}, u32[]{:S(2)}, u32[]{:S(2)}) %collective-permute-start.2) | collective-permute-done | bytes 262176 | tf_op jit(solution)/shard_map/ppermute | solution.py:27
  101.7 0.7 copy-done.19
  102.4 0.1 copy-done.20
  102.5 1.2 copy-done
  103.7 4.5 %shard_map.113 = (f32[256,256]{1,0:T(8,128)}, bf16[256,256]{1,0:T(8,128)(2,1)}, bf16[256,256]{1,0:T(8,128)(2,1)}, bf16[256,256]{1,0:T(8,128)(2,1)}) custom-call(s32[1]{0:T(128)} %bitcast.8.place_ref, bf16[256,512]{1,0:T(8,128)(2,1)} %get-tuple-element.25.refs_0_, bf16[256,512]{1,0:T(8,128)(2,1)} %copy-done.18, bf16[256,512]{1,0:T(8,128)(2,1)} %copy-done.19, ...), custom_call_target="tpu_custom_call" | custom-call | flops 1073741824 | bytes 4194304 | tf_op jit(solution)/shard_map/pallas_call | solution.py:119
  108.2 2.4 %collective-permute-start.8 = (bf16[256,256]{1,0:T(8,128)(2,1)}, bf16[256,256]{1,0:T(8,128)(2,1)S(1)}, u32[]{:S(2)}, u32[]{:S(2)}) collective-permute-start(bf16[256,256]{1,0:T(8,128)(2,1)} %get-tuple-element.28), channel_id=1, source_target_pairs={{0,8},{1,9},{2,10},{3,11},{4,12},{5,13},{6,14},{7,15},{8,0},{9,1},... | collective-permute-start | bytes 393224 | tf_op jit(solution)/shard_map/ppermute | solution.py:27
  110.7 1.1 collective-permute-start.9
  111.7 0.1 fusion.16
  111.9 0.2 copy.44
  112.0 0.8 reshape.85
  112.8 0.2 copy.45
  113.0 0.8 reshape.86
  113.8 0.7 copy-done.16
  114.5 0.7 copy-done.17
  115.2 4.5 %shard_map.114 = (f32[256,256]{1,0:T(8,128)}, bf16[256,256]{1,0:T(8,128)(2,1)}, bf16[256,256]{1,0:T(8,128)(2,1)}, bf16[256,256]{1,0:T(8,128)(2,1)}) custom-call(s32[1]{0:T(128)} %bitcast.8.place_ref, bf16[256,512]{1,0:T(8,128)(2,1)} %get-tuple-element.31.refs_0_, bf16[256,512]{1,0:T(8,128)(2,1)} %collective-permute-done.11.refs_1_, ...), custom_call_target="tpu_custom_call" | custom-call | flops 1073741824 | bytes 4194304 | tf_op jit(solution)/shard_map/pallas_call | solution.py:119
  119.8 1.6 %collective-permute-start.14 = (bf16[256,256]{1,0:T(8,128)(2,1)}, bf16[256,256]{1,0:T(8,128)(2,1)S(1)}, u32[]{:S(2)}, u32[]{:S(2)}) collective-permute-start(bf16[256,256]{1,0:T(8,128)(2,1)} %get-tuple-element.33), channel_id=1, source_target_pairs={{0,8},{1,9},{2,10},{3,11},{4,12},{5,13},{6,14},{7,15},{8,0},{9,1},... | collective-permute-start | bytes 393224 | tf_op jit(solution)/shard_map/ppermute | solution.py:27
  121.3 0.3 collective-permute-start.15
  121.7 1.6 %collective-permute-start.16 = (bf16[256,256]{1,0:T(8,128)(2,1)}, bf16[256,256]{1,0:T(8,128)(2,1)S(1)}, u32[]{:S(2)}, u32[]{:S(2)}) collective-permute-start(bf16[256,256]{1,0:T(8,128)(2,1)} %get-tuple-element.35), channel_id=1, source_target_pairs={{0,24},{1,25},{2,26},{3,27},{4,28},{5,29},{6,30},{7,31},{8,16},{9,... | collective-permute-start | bytes 393224 | tf_op jit(solution)/shard_map/ppermute | solution.py:27
  123.3 0.1 convert_add_fusion.1
  123.3 3.1 %collective-permute-done.14 = bf16[256,256]{1,0:T(8,128)(2,1)S(1)} collective-permute-done((bf16[256,256]{1,0:T(8,128)(2,1)}, bf16[256,256]{1,0:T(8,128)(2,1)S(1)}, u32[]{:S(2)}, u32[]{:S(2)}) %collective-permute-start.14) | collective-permute-done | bytes 131104 | tf_op jit(solution)/shard_map/ppermute | solution.py:27
  126.4 2.8 %collective-permute-done.15 = bf16[256,256]{1,0:T(8,128)(2,1)S(1)} collective-permute-done((bf16[256,256]{1,0:T(8,128)(2,1)}, bf16[256,256]{1,0:T(8,128)(2,1)S(1)}, u32[]{:S(2)}, u32[]{:S(2)}) %collective-permute-start.15) | collective-permute-done | bytes 131104 | tf_op jit(solution)/shard_map/ppermute | solution.py:27
  129.2 3.4 %collective-permute-done.16 = bf16[256,256]{1,0:T(8,128)(2,1)S(1)} collective-permute-done((bf16[256,256]{1,0:T(8,128)(2,1)}, bf16[256,256]{1,0:T(8,128)(2,1)S(1)}, u32[]{:S(2)}, u32[]{:S(2)}) %collective-permute-start.16) | collective-permute-done | bytes 131104 | tf_op jit(solution)/shard_map/ppermute | solution.py:27
  132.6 1.0 convert_add_fusion
  133.7 1.0 copy.46
  (58 shorter events, 0.3 us)
Async XLA Ops:
  3.5 12.2 %all-to-all-start = ((s32[16,1,1]{2,1,0:T(1,128)}), s32[16,1,1]{2,1,0:T(1,128)S(1)}, u32[]{:S(2)}, u32[]{:S(2)}) async-start(s32[16,1,1]{2,1,0:T(1,128)} %copy.41), calls=%async_computation | async-start | bytes 16384 | tf_op jit(solution)/shard_map/all_to_all | solution.py:315
  20.6 11.1 %copy-start.12 = (bf16[512,512]{1,0:T(8,128)(2,1)S(1)}, bf16[512,512]{1,0:T(8,128)(2,1)}, u32[]{:S(2)}) copy-start(bf16[512,512]{1,0:T(8,128)(2,1)} %param.12) | copy-start | bytes 1572868
  20.6 11.1 %copy-start.13 = (bf16[512,512]{1,0:T(8,128)(2,1)S(1)}, bf16[512,512]{1,0:T(8,128)(2,1)}, u32[]{:S(2)}) copy-start(bf16[512,512]{1,0:T(8,128)(2,1)} %d_ref.3) | copy-start | bytes 1572868
  20.7 17.9 %collective-permute-start.6 = (bf16[256,1024]{1,0:T(8,128)(2,1)S(1)}, bf16[256,1024]{1,0:T(8,128)(2,1)S(1)}, u32[]{:S(2)}, u32[]{:S(2)}) collective-permute-start(bf16[256,1024]{1,0:T(8,128)(2,1)S(1)} %pad_maximum_fusion.4), channel_id=1, source_target_pairs={{0,6},{1,7},{2,4},{3,5},{4,2},{5,3},{6,0},{7,1},{8,14},{9,15},{10,... | collective-permute-start | bytes 1572872 | tf_op jit(solution)/shard_map/ppermute | solution.py:27
  23.1 24.4 %collective-permute-start.5 = (bf16[256,1024]{1,0:T(8,128)(2,1)}, bf16[256,1024]{1,0:T(8,128)(2,1)S(1)}, u32[]{:S(2)}, u32[]{:S(2)}) collective-permute-start(bf16[256,1024]{1,0:T(8,128)(2,1)} %pad_maximum_fusion.3), channel_id=1, source_target_pairs={{0,4},{1,5},{2,6},{3,7},{4,0},{5,1},{6,2},{7,3},{8,12},{9,13},{10,... | collective-permute-start | bytes 1572872 | tf_op jit(solution)/shard_map/ppermute | solution.py:27
  25.4 22.1 %collective-permute-start.4 = (bf16[256,1024]{1,0:T(8,128)(2,1)}, bf16[256,1024]{1,0:T(8,128)(2,1)S(1)}, u32[]{:S(2)}, u32[]{:S(2)}) collective-permute-start(bf16[256,1024]{1,0:T(8,128)(2,1)} %pad_maximum_fusion.2), channel_id=1, source_target_pairs={{0,2},{1,3},{2,0},{3,1},{4,6},{5,7},{6,4},{7,5},{8,10},{9,11},{10,... | collective-permute-start | bytes 1572872 | tf_op jit(solution)/shard_map/ppermute | solution.py:27
  25.9 23.0 %all-to-all-start.1 = ((bf16[16,64,128]{2,1,0:T(8,128)(2,1)}), bf16[16,64,128]{2,1,0:T(8,128)(2,1)S(1)}, u32[]{:S(2)}, u32[]{:S(2)}) async-start(bf16[16,64,128]{2,1,0:T(8,128)(2,1)} %broadcast_select_fusion), calls=%async_computation.1 | async-start | bytes 524288 | tf_op jit(solution)/shard_map/all_to_all | solution.py:323
  38.6 20.1 %copy-start.1 = (bf16[256,1024]{1,0:T(8,128)(2,1)}, bf16[256,1024]{1,0:T(8,128)(2,1)S(1)}, u32[]{:S(2)}) copy-start(bf16[256,1024]{1,0:T(8,128)(2,1)S(1)} %collective-permute-done.6.refs_7_) | copy-start | bytes 1572868
  47.5 11.2 %copy-start.2 = (bf16[256,1024]{1,0:T(8,128)(2,1)}, bf16[256,1024]{1,0:T(8,128)(2,1)S(1)}, u32[]{:S(2)}) copy-start(bf16[256,1024]{1,0:T(8,128)(2,1)S(1)} %collective-permute-done.5.refs_6_) | copy-start | bytes 1572868
  47.5 11.2 %copy-start.3 = (bf16[256,1024]{1,0:T(8,128)(2,1)}, bf16[256,1024]{1,0:T(8,128)(2,1)S(1)}, u32[]{:S(2)}) copy-start(bf16[256,1024]{1,0:T(8,128)(2,1)S(1)} %collective-permute-done.4.refs_5_) | copy-start | bytes 1572868
  49.0 52.8 %collective-permute-start.7 = (bf16[3,256,1024]{2,1,0:T(8,128)(2,1)}, bf16[3,256,1024]{2,1,0:T(8,128)(2,1)S(1)}, u32[]{:S(2)}, u32[]{:S(2)}) collective-permute-start(bf16[3,256,1024]{2,1,0:T(8,128)(2,1)} %pad_maximum_fusion), channel_id=1, source_target_pairs={{0,1},{1,0},{2,3},{3,2},{4,5},{5,4},{6,7},{7,6},{8,9},{9,8},{10,11... | collective-permute-start | bytes 4718600 | tf_op jit(solution)/shard_map/ppermute | solution.py:27
  68.0 22.2 %copy-start.4 = (bf16[256,256]{1,0:T(8,128)(2,1)S(1)}, bf16[256,256]{1,0:T(8,128)(2,1)}, u32[]{:S(2)}) copy-start(bf16[256,256]{1,0:T(8,128)(2,1)} %get-tuple-element.72) | copy-start | bytes 393220
  68.0 22.2 %copy-start.5 = (bf16[256,256]{1,0:T(8,128)(2,1)S(1)}, bf16[256,256]{1,0:T(8,128)(2,1)}, u32[]{:S(2)}) copy-start(bf16[256,256]{1,0:T(8,128)(2,1)} %get-tuple-element.73) | copy-start | bytes 393220
  68.0 22.2 %copy-start.6 = (bf16[256,256]{1,0:T(8,128)(2,1)S(1)}, bf16[256,256]{1,0:T(8,128)(2,1)}, u32[]{:S(2)}) copy-start(bf16[256,256]{1,0:T(8,128)(2,1)} %get-tuple-element.74) | copy-start | bytes 393220
  68.0 22.2 %copy-start.7 = (bf16[256,256]{1,0:T(8,128)(2,1)S(1)}, bf16[256,256]{1,0:T(8,128)(2,1)}, u32[]{:S(2)}) copy-start(bf16[256,256]{1,0:T(8,128)(2,1)} %get-tuple-element.75) | copy-start | bytes 393220
  68.0 22.2 %copy-start.8 = (bf16[256,256]{1,0:T(8,128)(2,1)S(1)}, bf16[256,256]{1,0:T(8,128)(2,1)}, u32[]{:S(2)}) copy-start(bf16[256,256]{1,0:T(8,128)(2,1)} %get-tuple-element.76) | copy-start | bytes 393220
  68.1 22.2 %copy-start.9 = (bf16[256,256]{1,0:T(8,128)(2,1)S(1)}, bf16[256,256]{1,0:T(8,128)(2,1)}, u32[]{:S(2)}) copy-start(bf16[256,256]{1,0:T(8,128)(2,1)} %get-tuple-element.77) | copy-start | bytes 393220
  68.1 22.2 %copy-start.10 = (bf16[256,256]{1,0:T(8,128)(2,1)S(1)}, bf16[256,256]{1,0:T(8,128)(2,1)}, u32[]{:S(2)}) copy-start(bf16[256,256]{1,0:T(8,128)(2,1)} %get-tuple-element.78) | copy-start | bytes 393220
  68.1 22.2 %copy-start.11 = (bf16[256,256]{1,0:T(8,128)(2,1)S(1)}, bf16[256,256]{1,0:T(8,128)(2,1)}, u32[]{:S(2)}) copy-start(bf16[256,256]{1,0:T(8,128)(2,1)} %get-tuple-element.79) | copy-start | bytes 393220
  70.0 14.8 %all-to-all-start.2 = ((bf16[16,64,128]{2,1,0:T(8,128)(2,1)}), bf16[16,64,128]{2,1,0:T(8,128)(2,1)S(1)}, u32[]{:S(2)}, u32[]{:S(2)}) async-start(bf16[16,64,128]{2,1,0:T(8,128)(2,1)} %bitcast.7), calls=%async_computation.2 | async-start | bytes 524288 | tf_op jit(solution)/shard_map/all_to_all | solution.py:361
  85.1 9.6 %copy-start.15 = (bf16[256,512]{1,0:T(8,128)(2,1)S(1)}, bf16[256,512]{1,0:T(8,128)(2,1)}, u32[]{:S(2)}) copy-start(bf16[256,512]{1,0:T(8,128)(2,1)} %get-tuple-element.31.refs_0_) | copy-start | bytes 786436
  85.1 3.7 %collective-permute-start = (f32[8,64,128]{2,0,1:T(8,128)S(1)}, f32[8,64,128]{2,0,1:T(8,128)S(1)}, u32[]{:S(2)}, u32[]{:S(2)}) collective-permute-start(f32[8,64,128]{2,0,1:T(8,128)S(1)} %convolution_add_fusion), channel_id=1, source_target_pairs={{0,1},{1,0},{2,3},{3,2},{4,5},{5,4},{6,7},{7,6},{8,9},{9,8},{10,11... | collective-permute-start | bytes 786440 | tf_op jit(solution)/shard_map/ppermute | solution.py:27
  85.2 9.5 %collective-permute-start.1 = (bf16[256,512]{1,0:T(8,128)(2,1)}, bf16[256,512]{1,0:T(8,128)(2,1)S(1)}, u32[]{:S(2)}, u32[]{:S(2)}) collective-permute-start(bf16[256,512]{1,0:T(8,128)(2,1)} %get-tuple-element.25.refs_0_), channel_id=1, source_target_pairs={{0,2},{1,3},{2,0},{3,1},{4,6},{5,7},{6,4},{7,5},{8,10},{9,11},{10,... | collective-permute-start | bytes 786440 | tf_op jit(solution)/shard_map/ppermute | solution.py:27
  86.7 15.0 %collective-permute-start.2 = (bf16[256,512]{1,0:T(8,128)(2,1)}, bf16[256,512]{1,0:T(8,128)(2,1)S(1)}, u32[]{:S(2)}, u32[]{:S(2)}) collective-permute-start(bf16[256,512]{1,0:T(8,128)(2,1)} %get-tuple-element.25.refs_0_), channel_id=1, source_target_pairs={{0,4},{1,5},{2,6},{3,7},{4,0},{5,1},{6,2},{7,3},{8,12},{9,13},{10,... | collective-permute-start | bytes 786440 | tf_op jit(solution)/shard_map/ppermute | solution.py:27
  87.4 14.3 %collective-permute-start.3 = (bf16[256,512]{1,0:T(8,128)(2,1)}, bf16[256,512]{1,0:T(8,128)(2,1)S(1)}, u32[]{:S(2)}, u32[]{:S(2)}) collective-permute-start(bf16[256,512]{1,0:T(8,128)(2,1)} %get-tuple-element.25.refs_0_), channel_id=1, source_target_pairs={{0,6},{1,7},{2,4},{3,5},{4,2},{5,3},{6,0},{7,1},{8,14},{9,15},{10,... | collective-permute-start | bytes 786440 | tf_op jit(solution)/shard_map/ppermute | solution.py:27
  88.7 21.9 %collective-permute-start.11 = (bf16[256,512]{1,0:T(8,128)(2,1)}, bf16[256,512]{1,0:T(8,128)(2,1)}, u32[]{:S(2)}, u32[]{:S(2)}) collective-permute-start(bf16[256,512]{1,0:T(8,128)(2,1)} %get-tuple-element.31.refs_0_), channel_id=1, source_target_pairs={{0,2},{1,3},{2,0},{3,1},{4,6},{5,7},{6,4},{7,5},{8,10},{9,11},{10,... | collective-permute-start | bytes 786440 | tf_op jit(solution)/shard_map/ppermute | solution.py:27
  94.6 7.1 %copy-start.18 = (bf16[256,512]{1,0:T(8,128)(2,1)}, bf16[256,512]{1,0:T(8,128)(2,1)S(1)}, u32[]{:S(2)}) copy-start(bf16[256,512]{1,0:T(8,128)(2,1)S(1)} %collective-permute-done.1.refs_1_) | copy-start | bytes 786436
  94.6 19.1 %collective-permute-start.12 = (bf16[256,512]{1,0:T(8,128)(2,1)S(1)}, bf16[256,512]{1,0:T(8,128)(2,1)S(1)}, u32[]{:S(2)}, u32[]{:S(2)}) collective-permute-start(bf16[256,512]{1,0:T(8,128)(2,1)S(1)} %copy-done.15), channel_id=1, source_target_pairs={{0,4},{1,5},{2,6},{3,7},{4,0},{5,1},{6,2},{7,3},{8,12},{9,13},{10,... | collective-permute-start | bytes 786440 | tf_op jit(solution)/shard_map/ppermute | solution.py:27
  101.7 0.7 copy-start.19
  101.7 12.1 %collective-permute-start.13 = (bf16[256,512]{1,0:T(8,128)(2,1)S(1)}, bf16[256,512]{1,0:T(8,128)(2,1)S(1)}, u32[]{:S(2)}, u32[]{:S(2)}) collective-permute-start(bf16[256,512]{1,0:T(8,128)(2,1)S(1)} %copy-done.15), channel_id=1, source_target_pairs={{0,6},{1,7},{2,4},{3,5},{4,2},{5,3},{6,0},{7,1},{8,14},{9,15},{10,... | collective-permute-start | bytes 786440 | tf_op jit(solution)/shard_map/ppermute | solution.py:27
  101.7 0.8 copy-start.20
  102.5 1.2 copy-start
  108.2 13.4 %collective-permute-start.10 = (bf16[256,256]{1,0:T(8,128)(2,1)}, bf16[256,256]{1,0:T(8,128)(2,1)S(1)}, u32[]{:S(2)}, u32[]{:S(2)}) collective-permute-start(bf16[256,256]{1,0:T(8,128)(2,1)} %get-tuple-element.30), channel_id=1, source_target_pairs={{0,24},{1,25},{2,26},{3,27},{4,28},{5,29},{6,30},{7,31},{8,16},{9,... | collective-permute-start | bytes 393224 | tf_op jit(solution)/shard_map/ppermute | solution.py:27
  108.2 15.0 %collective-permute-start.8 = (bf16[256,256]{1,0:T(8,128)(2,1)}, bf16[256,256]{1,0:T(8,128)(2,1)S(1)}, u32[]{:S(2)}, u32[]{:S(2)}) collective-permute-start(bf16[256,256]{1,0:T(8,128)(2,1)} %get-tuple-element.28), channel_id=1, source_target_pairs={{0,8},{1,9},{2,10},{3,11},{4,12},{5,13},{6,14},{7,15},{8,0},{9,1},... | collective-permute-start | bytes 393224 | tf_op jit(solution)/shard_map/ppermute | solution.py:27
  110.7 12.6 %collective-permute-start.9 = (bf16[256,256]{1,0:T(8,128)(2,1)}, bf16[256,256]{1,0:T(8,128)(2,1)S(1)}, u32[]{:S(2)}, u32[]{:S(2)}) collective-permute-start(bf16[256,256]{1,0:T(8,128)(2,1)} %get-tuple-element.29), channel_id=1, source_target_pairs={{0,16},{1,17},{2,18},{3,19},{4,20},{5,21},{6,22},{7,23},{8,24},{9,... | collective-permute-start | bytes 393224 | tf_op jit(solution)/shard_map/ppermute | solution.py:27
  113.8 9.5 %copy-start.14 = (f32[256,256]{1,0:T(8,128)S(1)}, f32[256,256]{1,0:T(8,128)}, u32[]{:S(2)}) copy-start(f32[256,256]{1,0:T(8,128)} %get-tuple-element.27) | copy-start | bytes 786436
  113.8 0.7 copy-start.16
  114.5 0.7 copy-start.17
  119.8 6.6 %collective-permute-start.14 = (bf16[256,256]{1,0:T(8,128)(2,1)}, bf16[256,256]{1,0:T(8,128)(2,1)S(1)}, u32[]{:S(2)}, u32[]{:S(2)}) collective-permute-start(bf16[256,256]{1,0:T(8,128)(2,1)} %get-tuple-element.33), channel_id=1, source_target_pairs={{0,8},{1,9},{2,10},{3,11},{4,12},{5,13},{6,14},{7,15},{8,0},{9,1},... | collective-permute-start | bytes 393224 | tf_op jit(solution)/shard_map/ppermute | solution.py:27
  121.3 7.9 %collective-permute-start.15 = (bf16[256,256]{1,0:T(8,128)(2,1)}, bf16[256,256]{1,0:T(8,128)(2,1)S(1)}, u32[]{:S(2)}, u32[]{:S(2)}) collective-permute-start(bf16[256,256]{1,0:T(8,128)(2,1)} %get-tuple-element.34), channel_id=1, source_target_pairs={{0,16},{1,17},{2,18},{3,19},{4,20},{5,21},{6,22},{7,23},{8,24},{9,... | collective-permute-start | bytes 393224 | tf_op jit(solution)/shard_map/ppermute | solution.py:27
  121.7 11.0 %collective-permute-start.16 = (bf16[256,256]{1,0:T(8,128)(2,1)}, bf16[256,256]{1,0:T(8,128)(2,1)S(1)}, u32[]{:S(2)}, u32[]{:S(2)}) collective-permute-start(bf16[256,256]{1,0:T(8,128)(2,1)} %get-tuple-element.35), channel_id=1, source_target_pairs={{0,24},{1,25},{2,26},{3,27},{4,28},{5,29},{6,30},{7,31},{8,16},{9,... | collective-permute-start | bytes 393224 | tf_op jit(solution)/shard_map/ppermute | solution.py:27
where the time goes:
time: 137 us; the launch traced here: 135 us
  waiting for transfers between devices  42.5 us (31%)
  starting transfers between devices  35 us (26%)
  Pallas kernels  27.3 us (20%)
  local copies, waits for them, and re-layouts  15.3 us (11%)
  other arithmetic  11.9 us (9%)
  matrix products  1.58 us (1%)
    ppermute x17, waiting for transfers between devices, send(): return lax.ppermute(value, ('kv', 'tp'), perm)  31.6 us
    pallas_call x2, Pallas kernels, attention_backward(): pl.pallas_call(functools.partial(attention_kernel, head_dim, first, last,...  18.2 us
    ppermute x17, starting transfers between devices, send(): return lax.ppermute(value, ('kv', 'tp'), perm)  16.4 us
    pallas_call x2, Pallas kernels, weight_gradient(): pl.pallas_call(functools.partial(plane_kernel, outer, group), in_specs=[p...  9.08 us
    all_to_all x1, waiting for transfers between devices, shards(): lax.all_to_all(sent_back, 'kv', split_axis=0, concat_axis=0, tiled=True)  8.14 us
    all_to_all x1, starting transfers between devices, shards(): lax.all_to_all(wanted.reshape(peer_count, 1), 'kv', split_axis=0, concat_...  7.2 us
    unnamed x45, local copies, waits for them, and re-layouts  6.36 us
    all_to_all x1, starting transfers between devices, shards(): lax.all_to_all(sent_back, 'kv', split_axis=0, concat_axis=0, tiled=True)  5.7 us
  transfers between devices with their start and end apart: 20, of which 9 were waited for; matrix products, arithmetic and copies ran while one was open for 11% of the time, Pallas kernels for 20%

commit v1 on v0

--- a/solution.py
+++ b/solution.py
@@ -10,6 +10,8 @@
 from jax.sharding import PartitionSpec as P
 
 BLOCK = 64
+ATTEND_VMEM = 28 * 2**20
+PLANE_VMEM = 16 * 2**20
 STACK_UNROLL = 4
 BLOCK_UNROLL = 2
 
@@ -61,10 +63,9 @@
         columns_of(normed, partner(member, step, group), group, share * half, half)
         for step in range(1, group)
     ]
-    mine = [
-        columns_of(normed, member, group, first * half, half) for first in (share, 1 - share)
-    ]
-    return pieces, jnp.concatenate(mine, axis=0)
+    mine = [columns_of(normed, member, group, first * half, half) for first in (share, 1 - share)]
+    mine = jnp.concatenate(mine, axis=0)
+    return pieces, mine
 
 
 def exchange_normed(pieces):
@@ -73,7 +74,7 @@
         send(piece, flat_perm(step_perm(step, group, 1)))
         for step, piece in enumerate(pieces, start=1)
     ]
-    other = send(jnp.stack(got), flat_perm(lambda kv: kv, lambda tp: tp ^ 1))
+    other = [send(piece, flat_perm(lambda kv: kv, lambda tp: tp ^ 1)) for piece in got]
     return got, other
 
 
@@ -83,25 +84,20 @@
 
 
 def plane_kernel(outer, group, place_ref, *refs):
-    rights, mine_ref, others = refs[:group], refs[group], refs[group + 1:2 * group]
-    other_ref, own_ref, pieces = refs[2 * group], refs[2 * group + 1], refs[2 * group + 2:]
-    half = mine_ref.shape[0] // 2
+    rights, mine_ref = refs[:group], refs[group]
+    others, swapped = refs[group + 1:2 * group], refs[2 * group:3 * group - 1]
+    own_ref, pieces = refs[3 * group - 1], refs[3 * group:]
     width = mine_ref.shape[1] // outer
+    right = jnp.concatenate([ref[...] for ref in rights], axis=1)
     for step in range(outer):
         owner = partner(place_ref[0], step, outer)
         columns = pl.ds(pl.multiple_of(owner * width, width), width)
+        left = [mine_ref[:, columns]]
+        for first, second in zip(others, swapped):
+            left += [first[:, columns], second[:, columns]]
         total = jnp.dot(
-            rights[0][...], mine_ref[:, columns], preferred_element_type=jnp.float32
-        )
-        for i in range(group - 1):
-            total += jnp.dot(
-                rights[i + 1][:, :half], others[i][:, columns],
-                preferred_element_type=jnp.float32,
-            )
-            total += jnp.dot(
-                rights[i + 1][:, half:], other_ref[i, :, columns],
-                preferred_element_type=jnp.float32,
-            )
+            right, jnp.concatenate(left, axis=0), preferred_element_type=jnp.float32
+        )
         if step == 0:
             own_ref[...] = total
         else:
@@ -118,17 +114,18 @@
         in_vmem = pl.BlockSpec(memory_space=pltpu.VMEM)
         own, *pieces = pl.pallas_call(
             functools.partial(plane_kernel, outer, group),
-            in_specs=[pl.BlockSpec(memory_space=pltpu.SMEM)] + [in_vmem] * (2 * group + 1),
+            in_specs=[pl.BlockSpec(memory_space=pltpu.SMEM)] + [in_vmem] * (3 * group - 1),
             out_specs=[in_vmem] * outer,
             out_shape=[jax.ShapeDtypeStruct((columns, width), jnp.float32)] + [
                 jax.ShapeDtypeStruct((columns, width), jnp.bfloat16)
             ] * (outer - 1),
+            compiler_params=pltpu.CompilerParams(vmem_limit_bytes=PLANE_VMEM),
             cost_estimate=pl.CostEstimate(
                 flops=2 * columns * mine.size * group,
                 bytes_accessed=2 * group * mine.size,
                 transcendentals=0,
             ),
-        )(place.reshape(1).astype(jnp.int32), *rights, mine, *got, other)
+        )(place.reshape(1).astype(jnp.int32), *rights, mine, *got, *other)
     else:
         lefts = [mine]
         for i, piece in enumerate(got):
@@ -148,23 +145,13 @@
     return terms
 
 
-def sum_over_tp(value):
-    tp_size = lax.axis_size("tp")
-    step = 1
-    if tp_size & (tp_size - 1):
-        return lax.psum(value, "tp")
-    while step < tp_size:
-        value = value + send(value, flat_perm(lambda kv: kv, lambda tp: tp ^ step))
-        step *= 2
-    return value
-
-
 def attention_kernel(
     head_dim, first, last, part, share_ref, slot_ref, limit_ref, q_ref, d_ref, log_ref, sum_ref,
     table_ref, *rest,
 ):
     before_ref = None if first else rest[0]
-    dq_ref, turned_ref, sums_ref, stack_ref, dq_t_ref, lse_ref, delta_ref = rest[-7:]
+    sums_ref, stack_ref, dq_t_ref, lse_ref, delta_ref = rest[-5:]
+    dq_ref, turned_ref = rest[:2] if first else rest[1:3]
     blocks, slot_count = slot_ref.shape
     width = lse_ref.shape[2]
     half = width // 2
@@ -255,9 +242,12 @@
 
     lax.fori_loop(0, blocks // 2, write_two, 0, unroll=min(blocks // 2, STACK_UNROLL))
     if last:
-        sums = sums_ref[...]
-        low_columns = lax.broadcasted_iota(jnp.int32, sums.shape, 1) < head_dim
-        sums_ref[...] = jnp.where(low_columns, sums * score_scale, sums)
+        kept_ref, sent_ref = rest[-7:-5]
+        kept = kept_ref.shape[0]
+        low_columns = lax.broadcasted_iota(jnp.int32, (1, wide), 1) < head_dim
+        scales = jnp.where(low_columns, score_scale, 1.0)
+        kept_ref[...] = sums_ref[:kept] * scales
+        sent_ref[...] = (sums_ref[kept:] * scales).astype(jnp.bfloat16)
 
 
 def attention_backward(
@@ -274,8 +264,8 @@
     return pl.pallas_call(
         functools.partial(attention_kernel, head_dim, first, last, part),
         in_specs=[in_smem] * 3 + [in_vmem] * (5 if first else 6),
-        out_specs=[in_vmem] * 3,
-        scratch_shapes=[
+        out_specs=[in_vmem] * (4 if last else 3),
+        scratch_shapes=([pltpu.VMEM(table.shape, jnp.float32)] if last else []) + [
             pltpu.VMEM((blocks, 2 * heads * BLOCK, 2 * head_dim), jnp.bfloat16),
             pltpu.VMEM((blocks, head_dim, heads * BLOCK), jnp.float32),
             pltpu.VMEM((blocks, 1, heads * BLOCK), jnp.float32),
@@ -284,8 +274,11 @@
         out_shape=[
             jax.ShapeDtypeStruct((tok_rows, width), jnp.bfloat16),
             jax.ShapeDtypeStruct((width, tok_rows), jnp.bfloat16),
-            jax.ShapeDtypeStruct(table.shape, jnp.float32),
-        ],
+        ] + ([
+            jax.ShapeDtypeStruct((blocks * BLOCK, 2 * head_dim), jnp.float32),
+            jax.ShapeDtypeStruct((table.shape[0] - blocks * BLOCK, 2 * head_dim), jnp.bfloat16),
+        ] if last else [jax.ShapeDtypeStruct(table.shape, jnp.float32)]),
+        compiler_params=pltpu.CompilerParams(vmem_limit_bytes=ATTEND_VMEM),
         cost_estimate=pl.CostEstimate(
             flops=10 * tok_rows * slot_count * BLOCK * width,
             bytes_accessed=4 * tok_rows * width * 2,
@@ -319,7 +312,6 @@
     )
     picked = jnp.maximum(asked_for, 0)
     outgoing = jnp.take(pairs_local, picked, axis=0)
-    outgoing, normed = lax.optimization_barrier((outgoing, normed))
     fetched = lax.all_to_all(outgoing, "kv", split_axis=0, concat_axis=0, tiled=True)
     share = (lax.axis_index("tp") % 2).astype(jnp.int32)
     pieces, mine = regroup_normed(normed, share)
@@ -341,16 +333,15 @@
     sums = None
     gradients, rights = [], []
     for part in range(parts):
-        gradient, turned, sums = attention_backward(
+        gradient, turned, *sums = attention_backward(
             queries, cotangent, log_sum.T, deltas, table, share, slot_index, limits, part,
-            parts, sums,
+            parts, None if part == 0 else sums[0],
         )
         gradients.append(gradient)
         rights.append([turned] + gather_group(turned))
     query_gradient = jnp.concatenate(gradients, axis=1)
-    block_sums = sums.reshape(block_table.shape)
-    own_part = block_sums[:local_blocks]
-    sent_back = block_sums[local_blocks:].astype(jnp.bfloat16)
+    own_part = sums[0].reshape(local_blocks, BLOCK, 2 * head_dim)
+    sent_back = sums[1].reshape(peer_count, BLOCK, 2 * head_dim)
     taken_by = (asked_for[:, None] == jnp.arange(local_blocks, dtype=jnp.int32)[None, :]).astype(
         jnp.float32
     )
@@ -362,9 +353,15 @@
     totals = own_part + jnp.einsum(
         "sb,skc->bkc", taken_by, returned.astype(jnp.float32), precision=lax.Precision.HIGHEST
     )
-    totals = sum_over_tp(totals)
-    grad_keys = totals[:, :, :head_dim].reshape(tok_rows, head_dim)
-    grad_values = totals[:, :, head_dim:].reshape(tok_rows, head_dim)
+    tp_size = lax.axis_size("tp")
+    step = 2
+    while step < tp_size:
+        totals = totals + send(totals, flat_perm(lambda kv: kv, lambda tp: tp ^ step))
+        step *= 2
+    received = send(totals, flat_perm(lambda kv: kv, lambda tp: tp ^ 1))
+    totals = (totals + received).reshape(tok_rows, 2 * head_dim)
+    grad_keys = totals[:, :head_dim]
+    grad_values = totals[:, head_dim:]
     return (query_gradient, grad_keys, grad_values, weight_grad)
 
 

time: 137 us -> 110 us (0.80)
  the two profiles are of different devices: /device:TPU:10 before, /device:TPU:0 now
where the time goes in v1:
time: 110 us; the launch traced here: 109 us
  starting transfers between devices  41 us (37%)
  Pallas kernels  22.1 us (20%)
  waiting for transfers between devices  18.1 us (16%)
  local copies, waits for them, and re-layouts  11.8 us (11%)
  other arithmetic  11.2 us (10%)
  matrix products  3.76 us (3%)
    ppermute x19, starting transfers between devices, send(): return lax.ppermute(value, ('kv', 'tp'), perm)  22.3 us
    pallas_call x2, Pallas kernels, attention_backward(): pl.pallas_call(functools.partial(attention_kernel, head_dim, first, last,...  16 us
    ppermute x19, waiting for transfers between devices, send(): return lax.ppermute(value, ('kv', 'tp'), perm)  14.8 us
    all_to_all x1, starting transfers between devices, shards(): lax.all_to_all(wanted.reshape(peer_count, 1), 'kv', split_axis=0, concat_...  8.34 us
    unnamed x27, local copies, waits for them, and re-layouts  7.51 us
    pallas_call x2, Pallas kernels, weight_gradient(): pl.pallas_call(functools.partial(plane_kernel, outer, group), in_specs=[p...  6.12 us
    all_to_all x1, starting transfers between devices, shards(): lax.all_to_all(sent_back, 'kv', split_axis=0, concat_axis=0, tiled=True)  6.01 us
    all_to_all x1, starting transfers between devices, shards(): lax.all_to_all(outgoing, 'kv', split_axis=0, concat_axis=0, tiled=True)  4.37 us
  transfers between devices with their start and end apart: 22, of which 6 were waited for; matrix products, arithmetic and copies ran while one was open for 16% of the time, Pallas kernels for 20%

profile of v1, /device:TPU:0, one launch (start us, length us, event | category | flops | bytes accessed | tf_op | source)
XLA Modules:
  0.0 109.1 jit_solution(13363113131152239975)
XLA Ops:
  0.6 0.7 compare_and_fusion
  1.4 0.8 broadcast_add_fusion
  2.1 0.1 select_reduce_fusion
  2.2 0.7 copy.44
  2.9 8.3 %all-to-all-start = ((s32[16,1,1]{2,1,0:T(1,128)}), s32[16,1,1]{2,1,0:T(1,128)S(1)}, u32[]{:S(2)}, u32[]{:S(2)}) async-start(s32[16,1,1]{2,1,0:T(1,128)} %copy.44), calls=%async_computation | async-start | bytes 16384 | tf_op jit(solution)/shard_map/all_to_all | solution.py:308
  11.4 2.9 %fusion.15 = (bf16[256,256]{1,0:T(8,128)(2,1)S(1)}, bf16[256,256]{1,0:T(8,128)(2,1)S(1)}, bf16[256,256]{1,0:T(8,128)(2,1)S(1)}, bf16[256,256]{1,0:T(8,128)(2,1)S...) fusion(bf16[512,4096]{1,0:T(8,128)(2,1)} %param.8, ...), kind=kLoop, calls=%fused_computation.51 | loop fusion | bytes 5242952 | tf_op jit(solution)/shard_map/dynamic_slice | solution.py:52
  14.3 0.9 pad_maximum_fusion.1
  15.1 1.8 %collective-permute-start.4 = (bf16[256,1024]{1,0:T(8,128)(2,1)}, bf16[256,1024]{1,0:T(8,128)(2,1)S(1)}, u32[]{:S(2)}, u32[]{:S(2)}) collective-permute-start(bf16[256,1024]{1,0:T(8,128)(2,1)} %pad_maximum_fusion.1), channel_id=1, source_target_pairs={{0,2},{1,3},{2,0},{3,1},{4,6},{5,7},{6,4},{7,5},{8,10},{9,11},{10,... | collective-permute-start | bytes 1572872 | tf_op jit(solution)/shard_map/ppermute | solution.py:29
  16.9 0.1 copy.43
  17.1 0.1 copy.42
  17.2 0.0 copy-start
  17.2 0.1 pad_maximum_fusion.5
  17.3 1.2 %all-to-all-done = s32[16,1,1]{2,1,0:T(1,128)S(1)} async-done(((s32[16,1,1]{2,1,0:T(1,128)}), s32[16,1,1]{2,1,0:T(1,128)S(1)}, u32[]{:S(2)}, u32[]{:S(2)}) %all-to-all-start) | async-done | bytes 96 | tf_op jit(solution)/shard_map/all_to_all | solution.py:308
  18.5 0.7 add_reduce_fusion
  19.2 0.6 gather_fusion
  19.8 0.8 broadcast_select_fusion
  20.6 4.4 %all-to-all-start.1 = ((bf16[16,64,128]{2,1,0:T(8,128)(2,1)}), bf16[16,64,128]{2,1,0:T(8,128)(2,1)S(1)}, u32[]{:S(2)}, u32[]{:S(2)}) async-start(bf16[16,64,128]{2,1,0:T(8,128)(2,1)} %broadcast_select_fusion), calls=%async_computation.1 | async-start | bytes 524288 | tf_op jit(solution)/shard_map/all_to_all | solution.py:315
  25.0 0.0 copy-start.7
  25.0 0.9 pad_maximum_fusion.2
  25.9 1.9 %collective-permute-start.5 = (bf16[256,1024]{1,0:T(8,128)(2,1)}, bf16[256,1024]{1,0:T(8,128)(2,1)S(1)}, u32[]{:S(2)}, u32[]{:S(2)}) collective-permute-start(bf16[256,1024]{1,0:T(8,128)(2,1)} %pad_maximum_fusion.2), channel_id=1, source_target_pairs={{0,4},{1,5},{2,6},{3,7},{4,0},{5,1},{6,2},{7,3},{8,12},{9,13},{10,... | collective-permute-start | bytes 1572872 | tf_op jit(solution)/shard_map/ppermute | solution.py:29
  27.8 0.9 pad_maximum_fusion.3
  28.7 1.5 %collective-permute-start.6 = (bf16[256,1024]{1,0:T(8,128)(2,1)}, bf16[256,1024]{1,0:T(8,128)(2,1)S(1)}, u32[]{:S(2)}, u32[]{:S(2)}) collective-permute-start(bf16[256,1024]{1,0:T(8,128)(2,1)} %pad_maximum_fusion.3), channel_id=1, source_target_pairs={{0,6},{1,7},{2,4},{3,5},{4,2},{5,3},{6,0},{7,1},{8,14},{9,15},{10,... | collective-permute-start | bytes 1572872 | tf_op jit(solution)/shard_map/ppermute | solution.py:29
  30.1 1.7 %fusion.sum_ref = f32[8,512]{1,0:T(8,128)S(1)} fusion(bf16[512,512]{1,0:T(8,128)(2,1)} %param.12, bf16[512,512]{1,0:T(8,128)(2,1)S(1)} %copy-done, s32[512]{0:T(512)S(1)} %add_select_fusion.2), kind=kOutput, calls=%fused_computation.3 | convolution fusion | flops 25956352 | bytes 1067008 | tf_op jit(solution)/shard_map/dot_general | solution.py:327
  31.9 2.2 %all-to-all-done.1 = bf16[16,64,128]{2,1,0:T(8,128)(2,1)S(1)} async-done(((bf16[16,64,128]{2,1,0:T(8,128)(2,1)}), bf16[16,64,128]{2,1,0:T(8,128)(2,1)S(1)}, u32[]{:S(2)}, u32[]{:S(2)}) %all-to-all-start.1) | async-done | bytes 262176 | tf_op jit(solution)/shard_map/all_to_all | solution.py:315
  34.1 7.9 %shard_map.111 = (bf16[512,256]{1,0:T(8,128)(2,1)S(1)}, bf16[256,512]{1,0:T(8,128)(2,1)}, f32[1536,128]{1,0:T(8,128)S(1)}) custom-call(s32[1]{0:T(128)} %bitcast.share_ref, s32[8,16]{1,0:T(8,128)S(1)} %get-tuple-element.82.slot_ref, s32[8,16]{1,0:T(8,128)S(1)} %get-tuple-element.81.limit_ref, bf16[512,512]{1,0:T(8,128)(2,1)S(1)} %copy-done.7, ...), custom_call_target="tpu_custom_call" | custom-call | flops 1342177280 | bytes 1048576 | tf_op jit(solution)/shard_map/pallas_call | solution.py:264
  42.0 8.1 %shard_map.112 = (bf16[512,256]{1,0:T(8,128)(2,1)S(1)}, bf16[256,512]{1,0:T(8,128)(2,1)}, f32[512,128]{1,0:T(8,128)S(1)}, bf16[1024,128]{1,0:T(8,128)(2,1)}) custom-call(s32[1]{0:T(128)} %bitcast.share_ref, s32[8,16]{1,0:T(8,128)S(1)} %get-tuple-element.82.slot_ref, s32[8,16]{1,0:T(8,128)S(1)} %get-tuple-element.81.limit_ref, ...), custom_call_target="tpu_custom_call" | custom-call | flops 1342177280 | bytes 1048576 | tf_op jit(solution)/shard_map/pallas_call | solution.py:264
  50.1 0.7 copy-done.1
  50.8 0.7 copy-done.2
  51.5 1.3 %collective-permute-start.13 = (bf16[256,512]{1,0:T(8,128)(2,1)}, bf16[256,512]{1,0:T(8,128)(2,1)S(1)}, u32[]{:S(2)}, u32[]{:S(2)}) collective-permute-start(bf16[256,512]{1,0:T(8,128)(2,1)} %get-tuple-element.29.refs_0_), channel_id=1, source_target_pairs={{0,2},{1,3},{2,0},{3,1},{4,6},{5,7},{6,4},{7,5},{8,10},{9,11},{10,... | collective-permute-start | bytes 786440 | tf_op jit(solution)/shard_map/ppermute | solution.py:29
  52.7 0.3 collective-permute-start.14
  53.1 0.5 collective-permute-start.8
  53.6 0.1 collective-permute-start.9
  53.6 6.0 %all-to-all-start.2 = ((bf16[16,64,128]{2,1,0:T(8,128)(2,1)}), bf16[16,64,128]{2,1,0:T(8,128)(2,1)}, u32[]{:S(2)}, u32[]{:S(2)}) async-start(bf16[16,64,128]{2,1,0:T(8,128)(2,1)} %bitcast.7), calls=%async_computation.2 | async-start | bytes 524288 | tf_op jit(solution)/shard_map/all_to_all | solution.py:352
  59.7 0.7 copy-done.3
  60.4 2.8 %collective-permute-start.15 = (bf16[256,512]{1,0:T(8,128)(2,1)}, bf16[256,512]{1,0:T(8,128)(2,1)}, u32[]{:S(2)}, u32[]{:S(2)}) collective-permute-start(bf16[256,512]{1,0:T(8,128)(2,1)} %get-tuple-element.29.refs_0_), channel_id=1, source_target_pairs={{0,6},{1,7},{2,4},{3,5},{4,2},{5,3},{6,0},{7,1},{8,14},{9,15},{10,... | collective-permute-start | bytes 786440 | tf_op jit(solution)/shard_map/ppermute | solution.py:29
  63.1 0.7 copy-done.5
  63.8 0.6 collective-permute-start.1
  64.4 1.4 %maximum_maximum_fusion.refs_4_ = bf16[512,1024]{1,0:T(8,128)(2,1)S(1)} fusion(bf16[256,256]{1,0:T(8,128)(2,1)S(1)} %get-tuple-element.68, bf16[256,256]{1,0:T(8,128)(2,1)} %get-tuple-element.69, bf16[256,256]{1,0:T(8,128)(2,1)} %get-tuple-element.70, bf16[256,256]{1,0:T(8,128)(2,1)} %get-tuple-element.71, bf16[256,256]{1,0:T(8,128)(2,1)} %get-tuple-element.72, ...), kind=kLoop, calls=%fused_computation.2 | loop fusion | flops 8388608 | bytes 2097152 | tf_op jit(solution)/shard_map/concatenate | solution.py:67
  65.8 1.8 %pad_maximum_fusion = bf16[512,512]{1,0:T(8,128)(2,1)} fusion(bf16[512,256]{1,0:T(8,128)(2,1)} %copy-done.2, bf16[512,256]{1,0:T(8,128)(2,1)S(1)} %get-tuple-element.19), kind=kLoop, calls=%fused_computation.7 | loop fusion | flops 1048576 | bytes 1048576 | tf_op jit(solution)/shard_map/concatenate | solution.py:342
  67.6 5.1 %collective-permute-done.15.refs_3_ = bf16[256,512]{1,0:T(8,128)(2,1)} collective-permute-done((bf16[256,512]{1,0:T(8,128)(2,1)}, bf16[256,512]{1,0:T(8,128)(2,1)}, u32[]{:S(2)}, u32[]{:S(2)}) %collective-permute-start.15) | collective-permute-done | bytes 262176 | tf_op jit(solution)/shard_map/ppermute | solution.py:29
  72.7 1.5 %collective-permute-start.2 = (bf16[256,512]{1,0:T(8,128)(2,1)}, bf16[256,512]{1,0:T(8,128)(2,1)}, u32[]{:S(2)}, u32[]{:S(2)}) collective-permute-start(bf16[256,512]{1,0:T(8,128)(2,1)} %get-tuple-element.24.refs_0_), channel_id=1, source_target_pairs={{0,4},{1,5},{2,6},{3,7},{4,0},{5,1},{6,2},{7,3},{8,12},{9,13},{10,... | collective-permute-start | bytes 786440 | tf_op jit(solution)/shard_map/ppermute | solution.py:29
  74.1 1.5 %collective-permute-start.3 = (bf16[256,512]{1,0:T(8,128)(2,1)}, bf16[256,512]{1,0:T(8,128)(2,1)}, u32[]{:S(2)}, u32[]{:S(2)}) collective-permute-start(bf16[256,512]{1,0:T(8,128)(2,1)} %get-tuple-element.24.refs_0_), channel_id=1, source_target_pairs={{0,6},{1,7},{2,4},{3,5},{4,2},{5,3},{6,0},{7,1},{8,14},{9,15},{10,... | collective-permute-start | bytes 786440 | tf_op jit(solution)/shard_map/ppermute | solution.py:29
  75.6 0.9 copy-done.4
  76.6 0.9 copy-done.6
  77.5 3.3 %shard_map.114 = (f32[256,256]{1,0:T(8,128)S(1)}, bf16[256,256]{1,0:T(8,128)(2,1)S(1)}, bf16[256,256]{1,0:T(8,128)(2,1)}, bf16[256,256]{1,0:T(8,128)(2,1)}) custom-call(s32[1]{0:T(128)} %bitcast.9.place_ref, bf16[256,512]{1,0:T(8,128)(2,1)} %get-tuple-element.29.refs_0_, bf16[256,512]{1,0:T(8,128)(2,1)S(1)} %copy-done.4, bf16[256,512]{1,0:T(8,128)(2,1)S(1)} %copy-done.6, ...), custom_call_target="tpu_custom_call" | custom-call | flops 1073741824 | bytes 4194304 | tf_op jit(solution)/shard_map/pallas_call | solution.py:115
  80.9 3.0 %collective-permute-start.18 = (bf16[256,256]{1,0:T(8,128)(2,1)}, bf16[256,256]{1,0:T(8,128)(2,1)}, u32[]{:S(2)}, u32[]{:S(2)}) collective-permute-start(bf16[256,256]{1,0:T(8,128)(2,1)} %get-tuple-element.33), channel_id=1, source_target_pairs={{0,24},{1,25},{2,26},{3,27},{4,28},{5,29},{6,30},{7,31},{8,16},{9,... | collective-permute-start | bytes 393224 | tf_op jit(solution)/shard_map/ppermute | solution.py:29
  83.8 0.1 collective-permute-start.17
  84.0 1.3 %collective-permute-start.16 = (bf16[256,256]{1,0:T(8,128)(2,1)S(1)}, bf16[256,256]{1,0:T(8,128)(2,1)}, u32[]{:S(2)}, u32[]{:S(2)}) collective-permute-start(bf16[256,256]{1,0:T(8,128)(2,1)S(1)} %get-tuple-element.31), channel_id=1, source_target_pairs={{0,8},{1,9},{2,10},{3,11},{4,12},{5,13},{6,14},{7,15},{8,0},{9,1},... | collective-permute-start | bytes 393224 | tf_op jit(solution)/shard_map/ppermute | solution.py:29
  85.3 2.0 %convolution_add_fusion = f32[8,64,128]{2,0,1:T(8,128)} fusion(f32[8,64,128]{2,1,0:T(8,128)} %bitcast.16, bf16[16,64,128]{2,1,0:T(8,128)(2,1)} %all-to-all-done.2, s32[16]{0:T(128)S(1)} %get-tuple-element.54), kind=kOutput, calls=%fused_computation.1 | convolution fusion | flops 2162816 | bytes 786496 | tf_op jit(solution)/shard_map/sb,skc->bkc/dot_general | solution.py:353
  87.3 2.8 %shard_map.113 = (f32[256,256]{1,0:T(8,128)S(1)}, bf16[256,256]{1,0:T(8,128)(2,1)S(1)}, bf16[256,256]{1,0:T(8,128)(2,1)S(1)}, bf16[256,256]{1,0:T(8,128)(2,1)S(1)}) custom-call(s32[1]{0:T(128)} %bitcast.9.place_ref, bf16[256,512]{1,0:T(8,128)(2,1)} %get-tuple-element.24.refs_0_, bf16[256,512]{1,0:T(8,128)(2,1)} %collective-permute-done.1.refs_1_, ...), custom_call_target="tpu_custom_call" | custom-call | flops 1073741824 | bytes 4194304 | tf_op jit(solution)/shard_map/pallas_call | solution.py:115
  90.1 3.0 %collective-permute-start.12 = (bf16[256,256]{1,0:T(8,128)(2,1)S(1)}, bf16[256,256]{1,0:T(8,128)(2,1)S(1)}, u32[]{:S(2)}, u32[]{:S(2)}) collective-permute-start(bf16[256,256]{1,0:T(8,128)(2,1)S(1)} %get-tuple-element.28), channel_id=1, source_target_pairs={{0,24},{1,25},{2,26},{3,27},{4,28},{5,29},{6,30},{7,31},{8,16},{9,... | collective-permute-start | bytes 393224 | tf_op jit(solution)/shard_map/ppermute | solution.py:29
  93.1 1.2 %collective-permute-start.11 = (bf16[256,256]{1,0:T(8,128)(2,1)S(1)}, bf16[256,256]{1,0:T(8,128)(2,1)S(1)}, u32[]{:S(2)}, u32[]{:S(2)}) collective-permute-start(bf16[256,256]{1,0:T(8,128)(2,1)S(1)} %get-tuple-element.27), channel_id=1, source_target_pairs={{0,16},{1,17},{2,18},{3,19},{4,20},{5,21},{6,22},{7,23},{8,24},{9,... | collective-permute-start | bytes 393224 | tf_op jit(solution)/shard_map/ppermute | solution.py:29
  94.3 0.2 collective-permute-done.17
  94.5 0.1 collective-permute-start.10
  94.6 1.1 %convert_add_fusion = f32[256,256]{1,0:T(8,128)S(1)} fusion(bf16[256,256]{1,0:T(8,128)(2,1)} %collective-permute-done.18, bf16[256,256]{1,0:T(8,128)(2,1)} %collective-permute-done.17, f32[256,256]{1,0:T(8,128)S(1)} %get-tuple-element.30, bf16[256,256]{1,0:T(8,128)(2,1)} %collective-permute-done.16), kind=kLoop, calls=%fused_computation.14 | loop fusion | flops 393216 | bytes 917504 | tf_op jit(solution)/shard_map/add | solution.py:350
  95.7 2.8 %collective-permute-done.12 = bf16[256,256]{1,0:T(8,128)(2,1)S(1)} collective-permute-done((bf16[256,256]{1,0:T(8,128)(2,1)S(1)}, bf16[256,256]{1,0:T(8,128)(2,1)S(1)}, u32[]{:S(2)}, u32[]{:S(2)}) %collective-permute-start.12) | collective-permute-done | bytes 131104 | tf_op jit(solution)/shard_map/ppermute | solution.py:29
  98.4 6.7 %collective-permute-done.11 = bf16[256,256]{1,0:T(8,128)(2,1)S(1)} collective-permute-done((bf16[256,256]{1,0:T(8,128)(2,1)S(1)}, bf16[256,256]{1,0:T(8,128)(2,1)S(1)}, u32[]{:S(2)}, u32[]{:S(2)}) %collective-permute-start.11) | collective-permute-done | bytes 131104 | tf_op jit(solution)/shard_map/ppermute | solution.py:29
  105.2 0.1 convert_add_fusion.1
  105.3 1.0 copy.50
  106.3 1.1 add.202
  107.3 0.1 copy.47
  107.4 0.1 fusion.16
  107.5 0.8 copy.48
  108.3 0.8 copy.49
  (38 shorter events, 0.2 us)
Async XLA Ops:
  2.9 15.6 %all-to-all-start = ((s32[16,1,1]{2,1,0:T(1,128)}), s32[16,1,1]{2,1,0:T(1,128)S(1)}, u32[]{:S(2)}, u32[]{:S(2)}) async-start(s32[16,1,1]{2,1,0:T(1,128)} %copy.44), calls=%async_computation | async-start | bytes 16384 | tf_op jit(solution)/shard_map/all_to_all | solution.py:308
  11.4 5.5 %copy-start.9 = (bf16[512,64]{0,1:T(8,128)(2,1)S(1)}, bf16[512,64]{0,1:T(8,128)(2,1)}, u32[]{:S(2)}) copy-start(bf16[512,64]{0,1:T(8,128)(2,1)} %param.11) | copy-start | bytes 196612
  11.4 5.6 %copy-start.10 = (bf16[512,64]{0,1:T(8,128)(2,1)S(1)}, bf16[512,64]{0,1:T(8,128)(2,1)}, u32[]{:S(2)}) copy-start(bf16[512,64]{0,1:T(8,128)(2,1)} %param.10) | copy-start | bytes 196612
  15.1 37.9 %collective-permute-start.4 = (bf16[256,1024]{1,0:T(8,128)(2,1)}, bf16[256,1024]{1,0:T(8,128)(2,1)S(1)}, u32[]{:S(2)}, u32[]{:S(2)}) collective-permute-start(bf16[256,1024]{1,0:T(8,128)(2,1)} %pad_maximum_fusion.1), channel_id=1, source_target_pairs={{0,2},{1,3},{2,0},{3,1},{4,6},{5,7},{6,4},{7,5},{8,10},{9,11},{10,... | collective-permute-start | bytes 1572872 | tf_op jit(solution)/shard_map/ppermute | solution.py:29
  17.2 12.9 %copy-start = (bf16[512,512]{1,0:T(8,128)(2,1)S(1)}, bf16[512,512]{1,0:T(8,128)(2,1)}, u32[]{:S(2)}) copy-start(bf16[512,512]{1,0:T(8,128)(2,1)} %d_ref.3) | copy-start | bytes 1572868
  20.6 13.4 %all-to-all-start.1 = ((bf16[16,64,128]{2,1,0:T(8,128)(2,1)}), bf16[16,64,128]{2,1,0:T(8,128)(2,1)S(1)}, u32[]{:S(2)}, u32[]{:S(2)}) async-start(bf16[16,64,128]{2,1,0:T(8,128)(2,1)} %broadcast_select_fusion), calls=%async_computation.1 | async-start | bytes 524288 | tf_op jit(solution)/shard_map/all_to_all | solution.py:315
  25.0 9.1 %copy-start.7 = (bf16[512,512]{1,0:T(8,128)(2,1)S(1)}, bf16[512,512]{1,0:T(8,128)(2,1)}, u32[]{:S(2)}) copy-start(bf16[512,512]{1,0:T(8,128)(2,1)} %q_ref.3) | copy-start | bytes 1572868
  25.0 9.1 %copy-start.8 = (f32[512,8]{0,1:T(8,128)S(1)}, f32[512,8]{0,1:T(8,128)}, u32[]{:S(2)}) copy-start(f32[512,8]{0,1:T(8,128)} %param.14) | copy-start | bytes 49156
  25.9 27.2 %collective-permute-start.5 = (bf16[256,1024]{1,0:T(8,128)(2,1)}, bf16[256,1024]{1,0:T(8,128)(2,1)S(1)}, u32[]{:S(2)}, u32[]{:S(2)}) collective-permute-start(bf16[256,1024]{1,0:T(8,128)(2,1)} %pad_maximum_fusion.2), channel_id=1, source_target_pairs={{0,4},{1,5},{2,6},{3,7},{4,0},{5,1},{6,2},{7,3},{8,12},{9,13},{10,... | collective-permute-start | bytes 1572872 | tf_op jit(solution)/shard_map/ppermute | solution.py:29
  28.7 24.9 %collective-permute-start.6 = (bf16[256,1024]{1,0:T(8,128)(2,1)}, bf16[256,1024]{1,0:T(8,128)(2,1)S(1)}, u32[]{:S(2)}, u32[]{:S(2)}) collective-permute-start(bf16[256,1024]{1,0:T(8,128)(2,1)} %pad_maximum_fusion.3), channel_id=1, source_target_pairs={{0,6},{1,7},{2,4},{3,5},{4,2},{5,3},{6,0},{7,1},{8,14},{9,15},{10,... | collective-permute-start | bytes 1572872 | tf_op jit(solution)/shard_map/ppermute | solution.py:29
  50.1 0.7 copy-start.1
  50.8 0.7 copy-start.2
  51.5 8.2 %collective-permute-start.13 = (bf16[256,512]{1,0:T(8,128)(2,1)}, bf16[256,512]{1,0:T(8,128)(2,1)S(1)}, u32[]{:S(2)}, u32[]{:S(2)}) collective-permute-start(bf16[256,512]{1,0:T(8,128)(2,1)} %get-tuple-element.29.refs_0_), channel_id=1, source_target_pairs={{0,2},{1,3},{2,0},{3,1},{4,6},{5,7},{6,4},{7,5},{8,10},{9,11},{10,... | collective-permute-start | bytes 786440 | tf_op jit(solution)/shard_map/ppermute | solution.py:29
  52.7 10.4 %collective-permute-start.14 = (bf16[256,512]{1,0:T(8,128)(2,1)}, bf16[256,512]{1,0:T(8,128)(2,1)S(1)}, u32[]{:S(2)}, u32[]{:S(2)}) collective-permute-start(bf16[256,512]{1,0:T(8,128)(2,1)} %get-tuple-element.29.refs_0_), channel_id=1, source_target_pairs={{0,4},{1,5},{2,6},{3,7},{4,0},{5,1},{6,2},{7,3},{8,12},{9,13},{10,... | collective-permute-start | bytes 786440 | tf_op jit(solution)/shard_map/ppermute | solution.py:29
  53.0 21.1 %collective-permute-start.7 = (bf16[256,1024]{1,0:T(8,128)(2,1)S(1)}, bf16[256,1024]{1,0:T(8,128)(2,1)S(1)}, u32[]{:S(2)}, u32[]{:S(2)}) collective-permute-start(bf16[256,1024]{1,0:T(8,128)(2,1)S(1)} %collective-permute-done.4.refs_5_), channel_id=1, source_target_pairs={{0,1},{1,0},{2,3},{3,2},{4,5},{5,4},{6,7},{7,6},{8,9},{9,8},{10,11... | collective-permute-start | bytes 1572872 | tf_op jit(solution)/shard_map/ppermute | solution.py:29
  53.1 22.6 %collective-permute-start.8 = (bf16[256,1024]{1,0:T(8,128)(2,1)S(1)}, bf16[256,1024]{1,0:T(8,128)(2,1)}, u32[]{:S(2)}, u32[]{:S(2)}) collective-permute-start(bf16[256,1024]{1,0:T(8,128)(2,1)S(1)} %collective-permute-done.5.refs_6_), channel_id=1, source_target_pairs={{0,1},{1,0},{2,3},{3,2},{4,5},{5,4},{6,7},{7,6},{8,9},{9,8},{10,11... | collective-permute-start | bytes 1572872 | tf_op jit(solution)/shard_map/ppermute | solution.py:29
  53.6 22.1 %collective-permute-start.9 = (bf16[256,1024]{1,0:T(8,128)(2,1)S(1)}, bf16[256,1024]{1,0:T(8,128)(2,1)}, u32[]{:S(2)}, u32[]{:S(2)}) collective-permute-start(bf16[256,1024]{1,0:T(8,128)(2,1)S(1)} %collective-permute-done.6.refs_7_), channel_id=1, source_target_pairs={{0,1},{1,0},{2,3},{3,2},{4,5},{5,4},{6,7},{7,6},{8,9},{9,8},{10,11... | collective-permute-start | bytes 1572872 | tf_op jit(solution)/shard_map/ppermute | solution.py:29
  53.6 31.6 %all-to-all-start.2 = ((bf16[16,64,128]{2,1,0:T(8,128)(2,1)}), bf16[16,64,128]{2,1,0:T(8,128)(2,1)}, u32[]{:S(2)}, u32[]{:S(2)}) async-start(bf16[16,64,128]{2,1,0:T(8,128)(2,1)} %bitcast.7), calls=%async_computation.2 | async-start | bytes 524288 | tf_op jit(solution)/shard_map/all_to_all | solution.py:352
  59.7 0.7 copy-start.3
  60.4 12.3 %collective-permute-start.15 = (bf16[256,512]{1,0:T(8,128)(2,1)}, bf16[256,512]{1,0:T(8,128)(2,1)}, u32[]{:S(2)}, u32[]{:S(2)}) collective-permute-start(bf16[256,512]{1,0:T(8,128)(2,1)} %get-tuple-element.29.refs_0_), channel_id=1, source_target_pairs={{0,6},{1,7},{2,4},{3,5},{4,2},{5,3},{6,0},{7,1},{8,14},{9,15},{10,... | collective-permute-start | bytes 786440 | tf_op jit(solution)/shard_map/ppermute | solution.py:29
  63.1 0.7 copy-start.5
  63.8 20.1 %collective-permute-start.1 = (bf16[256,512]{1,0:T(8,128)(2,1)}, bf16[256,512]{1,0:T(8,128)(2,1)}, u32[]{:S(2)}, u32[]{:S(2)}) collective-permute-start(bf16[256,512]{1,0:T(8,128)(2,1)} %get-tuple-element.24.refs_0_), channel_id=1, source_target_pairs={{0,2},{1,3},{2,0},{3,1},{4,6},{5,7},{6,4},{7,5},{8,10},{9,11},{10,... | collective-permute-start | bytes 786440 | tf_op jit(solution)/shard_map/ppermute | solution.py:29
  72.7 14.6 %collective-permute-start.2 = (bf16[256,512]{1,0:T(8,128)(2,1)}, bf16[256,512]{1,0:T(8,128)(2,1)}, u32[]{:S(2)}, u32[]{:S(2)}) collective-permute-start(bf16[256,512]{1,0:T(8,128)(2,1)} %get-tuple-element.24.refs_0_), channel_id=1, source_target_pairs={{0,4},{1,5},{2,6},{3,7},{4,0},{5,1},{6,2},{7,3},{8,12},{9,13},{10,... | collective-permute-start | bytes 786440 | tf_op jit(solution)/shard_map/ppermute | solution.py:29
  74.1 13.2 %collective-permute-start.3 = (bf16[256,512]{1,0:T(8,128)(2,1)}, bf16[256,512]{1,0:T(8,128)(2,1)}, u32[]{:S(2)}, u32[]{:S(2)}) collective-permute-start(bf16[256,512]{1,0:T(8,128)(2,1)} %get-tuple-element.24.refs_0_), channel_id=1, source_target_pairs={{0,6},{1,7},{2,4},{3,5},{4,2},{5,3},{6,0},{7,1},{8,14},{9,15},{10,... | collective-permute-start | bytes 786440 | tf_op jit(solution)/shard_map/ppermute | solution.py:29
  75.6 1.0 copy-start.4
  76.6 0.9 copy-start.6
  80.9 12.3 %collective-permute-start.18 = (bf16[256,256]{1,0:T(8,128)(2,1)}, bf16[256,256]{1,0:T(8,128)(2,1)}, u32[]{:S(2)}, u32[]{:S(2)}) collective-permute-start(bf16[256,256]{1,0:T(8,128)(2,1)} %get-tuple-element.33), channel_id=1, source_target_pairs={{0,24},{1,25},{2,26},{3,27},{4,28},{5,29},{6,30},{7,31},{8,16},{9,... | collective-permute-start | bytes 393224 | tf_op jit(solution)/shard_map/ppermute | solution.py:29
  83.8 10.7 %collective-permute-start.17 = (bf16[256,256]{1,0:T(8,128)(2,1)}, bf16[256,256]{1,0:T(8,128)(2,1)}, u32[]{:S(2)}, u32[]{:S(2)}) collective-permute-start(bf16[256,256]{1,0:T(8,128)(2,1)} %get-tuple-element.32), channel_id=1, source_target_pairs={{0,16},{1,17},{2,18},{3,19},{4,20},{5,21},{6,22},{7,23},{8,24},{9,... | collective-permute-start | bytes 393224 | tf_op jit(solution)/shard_map/ppermute | solution.py:29
  84.0 10.6 %collective-permute-start.16 = (bf16[256,256]{1,0:T(8,128)(2,1)S(1)}, bf16[256,256]{1,0:T(8,128)(2,1)}, u32[]{:S(2)}, u32[]{:S(2)}) collective-permute-start(bf16[256,256]{1,0:T(8,128)(2,1)S(1)} %get-tuple-element.31), channel_id=1, source_target_pairs={{0,8},{1,9},{2,10},{3,11},{4,12},{5,13},{6,14},{7,15},{8,0},{9,1},... | collective-permute-start | bytes 393224 | tf_op jit(solution)/shard_map/ppermute | solution.py:29
  87.3 19.0 %collective-permute-start = (f32[8,64,128]{2,0,1:T(8,128)}, f32[8,64,128]{2,0,1:T(8,128)}, u32[]{:S(2)}, u32[]{:S(2)}) collective-permute-start(f32[8,64,128]{2,0,1:T(8,128)} %convolution_add_fusion), channel_id=1, source_target_pairs={{0,1},{1,0},{2,3},{3,2},{4,5},{5,4},{6,7},{7,6},{8,9},{9,8},{10,11... | collective-permute-start | bytes 786440 | tf_op jit(solution)/shard_map/ppermute | solution.py:29
  90.1 8.3 %collective-permute-start.12 = (bf16[256,256]{1,0:T(8,128)(2,1)S(1)}, bf16[256,256]{1,0:T(8,128)(2,1)S(1)}, u32[]{:S(2)}, u32[]{:S(2)}) collective-permute-start(bf16[256,256]{1,0:T(8,128)(2,1)S(1)} %get-tuple-element.28), channel_id=1, source_target_pairs={{0,24},{1,25},{2,26},{3,27},{4,28},{5,29},{6,30},{7,31},{8,16},{9,... | collective-permute-start | bytes 393224 | tf_op jit(solution)/shard_map/ppermute | solution.py:29
  93.1 12.0 %collective-permute-start.11 = (bf16[256,256]{1,0:T(8,128)(2,1)S(1)}, bf16[256,256]{1,0:T(8,128)(2,1)S(1)}, u32[]{:S(2)}, u32[]{:S(2)}) collective-permute-start(bf16[256,256]{1,0:T(8,128)(2,1)S(1)} %get-tuple-element.27), channel_id=1, source_target_pairs={{0,16},{1,17},{2,18},{3,19},{4,20},{5,21},{6,22},{7,23},{8,24},{9,... | collective-permute-start | bytes 393224 | tf_op jit(solution)/shard_map/ppermute | solution.py:29
  94.5 10.7 %collective-permute-start.10 = (bf16[256,256]{1,0:T(8,128)(2,1)S(1)}, bf16[256,256]{1,0:T(8,128)(2,1)S(1)}, u32[]{:S(2)}, u32[]{:S(2)}) collective-permute-start(bf16[256,256]{1,0:T(8,128)(2,1)S(1)} %get-tuple-element.26), channel_id=1, source_target_pairs={{0,8},{1,9},{2,10},{3,11},{4,12},{5,13},{6,14},{7,15},{8,0},{9,1},... | collective-permute-start | bytes 393224 | tf_op jit(solution)/shard_map/ppermute | solution.py:29
